TPU v7x, 512 devices: a 8x2x16 block of a 8x8x16 slice. The times are simulated.
512 devices in a mesh: grp: 2 (over y), sp: 16 (over z), tp: 16 (over x, core).
Axes of the slice: x: 8, y: 2, z: 16, core: 2. Of those that a mesh axis runs over, the one named last changes fastest.
The devices are a block of a 8x8x16 slice.
Arguments:
- latent: bfloat16 [16384, 4096], P(('grp', 'sp'), 'tp'), parts along dimension 0, may hold values from -42 to 42
- context: bfloat16 [2048, 4096], P(('grp', 'sp'), 'tp'), parts along dimension 0, may hold values from -42 to 42
- conditions: float32 [4, 4096], P('grp', 'sp'), parts along dimension 0, may hold values from -6 to 6
- mod_weight: bfloat16 [4096, 3, 4096], P('sp', None, 'tp'), may hold values from -0.09375 to 0.09375
- norm_gain: float32 [4096], P('tp'), may hold values from 0.1 to 1.9
- w_query: bfloat16 [4096, 2048], P(None, 'tp'), may hold values from -0.09375 to 0.09375
- w_key: bfloat16 [4096, 2048], P(None, 'tp'), may hold values from -0.09375 to 0.09375
- w_value: bfloat16 [4096, 2048], P(None, 'tp'), may hold values from -0.09375 to 0.09375
- query_gain: float32 [64], replicated, may hold values from 1 to 14
- key_gain: float32 [64], replicated, may hold values from 1 to 14
- lambdas: float32 [16], P('tp'), may hold values from 0.3 to 0.8
- out_gain: float32 [128], replicated, may hold values from 0.1 to 1.9
- w_out: bfloat16 [2048, 4096], P(None, 'tp'), may hold values from -0.125 to 0.125
Outputs:
- updated: bfloat16 [16384, 4096], P(('grp', 'sp'), 'tp'), parts along dimension 0
There are 2 independent parts, one for each index of `grp`. A program takes and returns all parts, laid end to end along the dimension named above; an argument that names none is the same for every part. Nothing has to cross between parts.
All inputs are finite; a program needn't handle non-finite values.
Results may differ from a plain program's by a relative error of at most 0.0076.
Values may be sent and summed in bfloat16 or wider, within the bound.
A program may use at most 64 MiB of HBM per device.

v0:
```python
import math

import jax
import jax.numpy as jnp
from jax import lax
from jax.sharding import PartitionSpec as P

DK = 64
DV = 128
GRID_W = 64


epsilon = 1e-06


def sent_to_all(value, axis):
    size = lax.axis_size(axis)
    return lax.all_to_all(
        jnp.broadcast_to(value[None], (size, *value.shape)), axis, 0, 0, tiled=True
    )


def of_everyone(value, axis):
    everything = sent_to_all(value, axis)
    return jnp.sum(everything, axis=0)


def in_one_piece(arrays, axis, dim, along):
    both = jnp.concatenate(arrays, axis=along)
    whole, at, gathered = (lax.all_gather(both, axis, axis=dim, tiled=True), 0, [])
    for a in arrays:
        gathered.append(lax.slice_in_dim(whole, at, at + a.shape[along], axis=along))
        at += a.shape[along]
    return tuple(gathered)


def turn_half(halves, angles):
    quarter = halves.shape[-1] // 2
    cosine = jnp.cos(angles)[:, None, None, :]
    sine_part = jnp.sin(angles)[:, None, None, :]
    first_part = halves[..., :quarter]
    second = halves[..., quarter:]
    return jnp.concatenate(
        [first_part * cosine - second * sine_part, first_part * sine_part + second * cosine],
        axis=-1,
    )


def rotate(features, positions):
    half_width = features.shape[-1] // 2
    quarter = half_width // 2
    inverse = 10000.0 ** (-2.0 * jnp.arange(quarter, dtype=jnp.float32) / half_width)
    grid_row = (positions // GRID_W).astype(jnp.float32)
    grid_column = (positions % GRID_W).astype(jnp.float32)
    return jnp.concatenate(
        [
            turn_half(features[..., :half_width], grid_row[:, None] * inverse),
            turn_half(features[..., half_width:], grid_column[:, None] * inverse),
        ],
        axis=-1,
    )


def head_norm(features, gain_row):
    return (
        features
        * lax.rsqrt(jnp.mean(features * features, axis=-1, keepdims=True) + epsilon)
        * gain_row
    )


def modulate(rows_in, gain_row, shift_row, scale_row):
    floats = rows_in.astype(jnp.float32)
    factor = lax.rsqrt(jnp.mean(floats * floats, axis=1, keepdims=True) + epsilon)
    return (floats * factor * gain_row * (1.0 + scale_row) + shift_row).astype(jnp.bfloat16)


def local(
    latent,
    context,
    conditions,
    mod_weight,
    norm_gain,
    w_query,
    w_key,
    w_value,
    query_gain,
    key_gain,
    lambdas,
    out_gain,
    w_out,
):
    tok_rows = latent.shape[0]
    ctx_rows = context.shape[0]
    columns = latent.shape[1]
    heads_here = lambdas.shape[0]
    in_rows = mod_weight.shape[0]
    activated = jax.nn.silu(conditions).astype(jnp.bfloat16)
    partial_mod = jnp.dot(
        activated, mod_weight.reshape(in_rows, 3 * columns), preferred_element_type=jnp.float32
    ).reshape(2, 3, columns)
    modulation = of_everyone(partial_mod, "sp")
    lat_floats = latent.astype(jnp.float32)
    full_gain, full_pairs = (
        lax.all_gather(norm_gain, "tp", axis=0, tiled=True),
        lax.all_gather(modulation[:, :2], "tp", axis=2, tiled=True),
    )
    whole_lat, whole_ctx = in_one_piece((latent, context), "tp", 1, 0)
    hidden = modulate(whole_lat, full_gain, full_pairs[0, 0], full_pairs[0, 1])
    hidden_ctx = modulate(whole_ctx, full_gain, full_pairs[1, 0], full_pairs[1, 1])
    query_raw = jnp.dot(hidden, w_query, preferred_element_type=jnp.float32)
    key_raw = jnp.dot(hidden, w_key, preferred_element_type=jnp.float32)
    value_raw = jnp.dot(hidden, w_value, preferred_element_type=jnp.float32)
    ctx_key_raw = jnp.dot(hidden_ctx, w_key, preferred_element_type=jnp.float32)
    ctx_value_raw = jnp.dot(hidden_ctx, w_value, preferred_element_type=jnp.float32)
    positions = lax.axis_index("sp") * tok_rows + jnp.arange(tok_rows, dtype=jnp.int32)
    queries = rotate(
        head_norm(query_raw.reshape(tok_rows, heads_here, 2, DK), query_gain), positions
    ).astype(jnp.bfloat16)
    lat_keys = (
        rotate(head_norm(key_raw.reshape(tok_rows, heads_here, 2, DK), key_gain), positions)
        .astype(jnp.bfloat16)
        .reshape(tok_rows, heads_here * 2 * DK)
    )
    lat_values = value_raw.astype(jnp.bfloat16)
    ctx_keys = (
        head_norm(ctx_key_raw.reshape(ctx_rows, heads_here, 2, DK), key_gain)
        .astype(jnp.bfloat16)
        .reshape(ctx_rows, heads_here * 2 * DK)
    )
    ctx_values = ctx_value_raw.astype(jnp.bfloat16)
    scaling = DK ** (-0.5)

    def absorb(carried, key_rows, value_rows):
        key_count = key_rows.shape[0]
        key_block = key_rows.reshape(key_count, heads_here, 2, DK)
        value_block = value_rows.reshape(key_count, heads_here, DV)
        running_max, totals, weighted = carried
        scores = (
            jnp.einsum("qhmd,khmd->qhmk", queries, key_block, preferred_element_type=jnp.float32)
            * scaling
        )
        new_max = jnp.maximum(running_max, jnp.max(scores, axis=-1))
        rescale = jnp.exp(running_max - new_max)
        exponent = jnp.exp(scores - new_max[..., None])
        totals = totals * rescale + jnp.sum(exponent, axis=-1)
        weighted = weighted * rescale[..., None] + jnp.einsum(
            "qhmk,khv->qhmv",
            exponent.astype(jnp.bfloat16),
            value_block,
            preferred_element_type=jnp.float32,
        )
        return (new_max, totals, weighted)

    def absorb_rows(carried, key_rows, value_rows):
        key_count = key_rows.shape[0]
        block_rows = math.gcd(key_count, 512)

        def visit_block(block_index, partial_value):
            first_row = block_index * block_rows
            return absorb(
                partial_value,
                lax.dynamic_slice_in_dim(key_rows, first_row, block_rows, 0),
                lax.dynamic_slice_in_dim(value_rows, first_row, block_rows, 0),
            )

        return lax.fori_loop(0, key_count // block_rows, visit_block, carried)

    initial_state = (
        jnp.full((tok_rows, heads_here, 2), -1e30, jnp.float32),
        jnp.zeros((tok_rows, heads_here, 2), jnp.float32),
        jnp.zeros((tok_rows, heads_here, 2, DV), jnp.float32),
    )
    every_ctx_keys, every_ctx_values = in_one_piece((ctx_keys, ctx_values), "sp", 0, 1)
    carried = absorb_rows(initial_state, every_ctx_keys, every_ctx_values)
    pieces = in_one_piece((lat_keys, lat_values), "sp", 0, 1)
    carried = absorb_rows(carried, pieces[0], pieces[1])
    running_max, totals, weighted = carried
    attended = (
        weighted[:, :, 0] / totals[:, :, 0, None]
        - lambdas[None, :, None] * weighted[:, :, 1] / totals[:, :, 1, None]
    )
    head_out = head_norm(attended, out_gain).astype(jnp.bfloat16).reshape(tok_rows, heads_here * DV)
    mixed_rows = jnp.dot(
        lax.all_gather(head_out, "tp", axis=1, tiled=True),
        w_out,
        preferred_element_type=jnp.float32,
    )
    return (lat_floats + modulation[0, 2] * mixed_rows).astype(jnp.bfloat16)


def solution(mesh):
    in_specs = (
        P(("grp", "sp"), "tp"),
        P(("grp", "sp"), "tp"),
        P("grp", "sp"),
        P("sp", None, "tp"),
        P("tp"),
        P(None, "tp"),
        P(None, "tp"),
        P(None, "tp"),
        P(),
        P(),
        P("tp"),
        P(),
        P(None, "tp"),
    )
    out_specs = P(("grp", "sp"), "tp")
    return jax.shard_map(local, mesh=mesh, in_specs=in_specs, out_specs=out_specs, check_vma=False)
```

profile of v0, /device:TPU:65, one launch (start us, length us, event | category | flops | bytes accessed | tf_op | source)
XLA Modules:
  0.0 304.0 jit_solution(5467779890000573192)
XLA Ops:
  6.6 1.8 pad_maximum_fusion
  11.2 44.2 %all-to-all-start = ((f32[16,2,3,256]{3,1,2,0:T(2,128)}), f32[16,2,3,256]{3,1,2,0:T(2,128)S(1)}, u32[]{:S(2)}, u32[]{:S(2)}) async-start(f32[16,2,3,256]{3,1,2,0:T(2,128)} %broadcast_in_dim.16), calls=%async_computation | async-start | bytes 196608 | tf_op jit(solution)/shard_map/all_to_all | solution.py:18
  55.5 18.9 %all-gather = f32[16,1,256]{2,1,0:T(1,128)S(1)} all-gather(f32[1,1,256]{2,1,0:T(1,128)S(1)} %bitcast.220), channel_id=1, replica_groups=mesh['grp'=2,'sp'=16,'tp'=16] {'tp'}, dimensions={0}, use_global_device_ids=true | all-gather | bytes 17408 | tf_op jit(solution)/shard_map/all_gather | solution.py:105
  74.8 15.3 %all_gather.20 = f32[2,2,4096]{2,0,1:T(2,128)S(1)} all-gather(f32[2,2,256]{2,0,1:T(2,128)S(1)} %slice.110), channel_id=1, replica_groups=mesh['grp'=2,'sp'=16,'tp'=16] {'tp'}, dimensions={2}, use_global_device_ids=true | all-gather | bytes 69632 | tf_op jit(solution)/shard_map/all_gather | solution.py:106
  90.2 13.1 %all-gather.5.cloned.1.call-done = bf16[576,4096]{1,0:T(8,128)(2,1)} async-done(((bf16[576,256]{1,0:T(8,128)(2,1)}), bf16[576,4096]{1,0:T(8,128)(2,1)}) %all-gather.5.cloned.1.call-update) | async-done | bytes 4718608 | tf_op jit(solution)/shard_map/all_gather | solution.py:30
  103.3 3.1 %fusion.30 = f32[512]{0:T(512)S(1)} fusion(bf16[576,4096]{1,0:T(8,128)(2,1)} %all-gather.5.cloned.1.call-done), kind=kLoop, calls=%fused_computation.47 | loop fusion | flops 6290944 | bytes 4196352 | tf_op jit(solution)/shard_map/reduce_sum | solution.py:74
  106.4 3.4 %fusion.34 = bf16[512,4096]{1,0:T(8,128)(2,1)S(1)} fusion(f32[4096]{0:T(1024)S(1)} %bitcast.211, f32[4096]{0:T(1024)S(1)} %bitcast.210, f32[4096]{0:T(1024)S(1)} %bitcast.207, f32[512]{0:T(512)S(1)} %add_rsqrt_fusion.4, bf16[576,4096]{1,0:T(8,128)(2,1)} %all-gather.5.cloned.1.call-done), kind=kLoop, calls=%fused_computation.51 | loop fusion | flops 12582912 | bytes 8439808 | tf_op jit(solution)/shard_map/convert_element_type | solution.py:75
  109.8 1.5 convolution_convert_fusion
  116.5 1.8 fusion.66
  118.8 1.5 convolution_convert_fusion.1
  120.4 3.7 %fusion.67 = f32[512,128]{0,1:T(8,128)S(1)} fusion(bf16[512,4096]{1,0:T(8,128)(2,1)} %copy-done.1, bf16[4096,128]{1,0:T(8,128)(2,1)S(1)} %copy-done.4), kind=kOutput, calls=%fused_computation.130 | convolution fusion | flops 536870912 | bytes 5505024 | tf_op jit(solution)/shard_map/dot_general | solution.py:111
  124.3 29.9 %all_gather.21 = bf16[1024,256]{1,0:T(8,128)(2,1)S(1)} all-gather(bf16[64,256]{1,0:T(8,128)(2,1)S(1)} %pad_maximum_fusion.4), channel_id=1, replica_groups=mesh['grp'=2,'sp'=16,'tp'=16] {'sp'}, dimensions={0}, use_global_device_ids=true | all-gather | bytes 557056 | tf_op jit(solution)/shard_map/all_gather | solution.py:30
  154.2 3.5 %while.36 = (s32[]{:T(128)}, f32[512,1,2]{0,2,1:T(2,128)S(1)}, f32[512,1,2]{0,2,1:T(2,128)S(1)}, f32[512,1,2,128]{0,3,2,1:T(8,128)S(1)}, bf16[1024,128]{1,0:T(8,...) while((s32[]{:T(128)}, f32[512,1,2]{0,2,1:T(2,128)S(1)}, ...), condition=%wide.region_8.9_spmd.clone, body=%wide.region_5.8_spmd.clone.sunk | while | flops 205920256 | bytes 8323255 | solution.py:167
  157.7 28.5 %all-gather.7.cloned.1.call-done = bf16[8192,256]{0,1:T(8,128)(2,1)} async-done(((bf16[512,256]{0,1:T(8,128)(2,1)}), bf16[8192,256]{0,1:T(8,128)(2,1)}) %all-gather.7.cloned.1.call-update) | async-done | bytes 4194320 | tf_op jit(solution)/shard_map/all_gather | solution.py:30
  186.2 4.6 %fusion.63 = (bf16[8192,128]{0,1:T(8,128)(2,1)}, bf16[8192,128]{0,1:T(8,128)(2,1)}) fusion(bf16[8192,256]{0,1:T(8,128)(2,1)} %all-gather.7.cloned.1.call-done), kind=kLoop, calls=%fused_computation.126 | loop fusion | bytes 8388608 | tf_op jit(solution)/shard_map/slice | solution.py:32
  190.8 54.4 %while.35 = (s32[]{:T(128)}, f32[512,1,2]{0,2,1:T(2,128)S(1)}, f32[512,1,2]{0,2,1:T(2,128)S(1)}, f32[512,1,2,128]{0,3,2,1:T(8,128)S(1)}, bf16[8192,128]{0,1:T(8,...) while((s32[]{:T(128)}, f32[512,1,2]{0,2,1:T(2,128)S(1)}, ...), condition=%wide.region_13.14_spmd, body=%wide.region_10.13_spmd.sunk | while | flops 205786112 | bytes 8061091 | solution.py:167
  192.7 1.5 fusion.98
  196.1 1.5 fusion.98
  199.5 1.5 fusion.98
  202.9 1.5 fusion.98
  206.3 1.5 fusion.98
  209.7 1.5 fusion.98
  213.1 1.5 fusion.98
  216.5 1.5 fusion.98
  219.9 1.5 fusion.98
  223.2 1.5 fusion.98
  230.0 1.5 fusion.98
  233.4 1.5 fusion.98
  236.8 1.5 fusion.98
  243.6 1.5 fusion.98
  246.1 48.3 %all-gather.9.cloned.1.call-done = bf16[512,2048]{0,1:T(8,128)(2,1)} async-done(((bf16[512,128]{0,1:T(8,128)(2,1)}), bf16[512,2048]{0,1:T(8,128)(2,1)}) %all-gather.9.cloned.1.call-update) | async-done | bytes 2097168 | tf_op jit(solution)/shard_map/all_gather | solution.py:185
  294.4 3.1 %fusion.36 = bf16[512,256]{1,0:T(8,128)(2,1)} fusion(bf16[512,2048]{0,1:T(8,128)(2,1)} %all-gather.9.cloned.1.call-done, bf16[2048,256]{1,0:T(8,128)(2,1)S(1)} %copy-done, bf16[512,256]{1,0:T(8,128)(2,1)S(1)} %copy-done.5, f32[256]{0:T(256)S(1)} %bitcast.221), kind=kOutput, calls=%fused_computation.56 | convolution fusion | flops 537395200 | bytes 3671040 | tf_op jit(solution)/shard_map/dot_general | solution.py:184
  (183 shorter events, 44.8 us)
Async XLA Ops:
  6.5 287.9 %copy-start = (bf16[2048,256]{1,0:T(8,128)(2,1)S(1)}, bf16[2048,256]{1,0:T(8,128)(2,1)}, u32[]{:S(2)}) copy-start(bf16[2048,256]{1,0:T(8,128)(2,1)} %param.29) | copy-start | bytes 3145732
  6.6 49.0 %copy-start.6 = (f32[256]{0:T(256)S(1)}, f32[256]{0:T(256)}, u32[]{:S(2)}) copy-start(f32[256]{0:T(256)} %param.21) | copy-start | bytes 3076
  6.6 96.7 %all-gather.5.cloned.1.call-start = ((), (), s32[]{:S(2)}) async-start(), calls=%async_computation.1 | async-start | bytes 5013504 | tf_op jit(solution)/shard_map/all_gather | solution.py:30
  11.2 63.6 %all-to-all-start = ((f32[16,2,3,256]{3,1,2,0:T(2,128)}), f32[16,2,3,256]{3,1,2,0:T(2,128)S(1)}, u32[]{:S(2)}, u32[]{:S(2)}) async-start(f32[16,2,3,256]{3,1,2,0:T(2,128)} %broadcast_in_dim.16), calls=%async_computation | async-start | bytes 196608 | tf_op jit(solution)/shard_map/all_to_all | solution.py:18
  55.4 130.8 %all-gather.7.cloned.1.call-start = ((), (), s32[]{:S(2)}) async-start(), calls=%async_computation.2 | async-start | bytes 4456448 | tf_op jit(solution)/shard_map/all_gather | solution.py:30
  106.4 3.4 %copy-start.2 = (bf16[4096,128]{1,0:T(8,128)(2,1)S(1)}, bf16[4096,128]{1,0:T(8,128)(2,1)}, u32[]{:S(2)}) copy-start(bf16[4096,128]{1,0:T(8,128)(2,1)} %param.24) | copy-start | bytes 3145732
  109.8 2.0 copy-start.1
  109.8 2.0 copy-start.3
  111.8 1.6 copy-start.7
  114.4 180.1 %all-gather.9.cloned.1.call-start = ((), (), s32[]{:S(2)}) async-start(), calls=%async_computation.3 | async-start | bytes 2228224 | tf_op jit(solution)/shard_map/all_gather | solution.py:185
  118.8 1.6 copy-start.4
  120.4 3.8 %copy-start.8 = (f32[64]{0:T(128)S(1)}, f32[64]{0:T(128)}, u32[]{:S(2)}) copy-start(f32[64]{0:T(128)} %param.25) | copy-start | bytes 772
  190.8 54.5 %copy-start.9 = (f32[128]{0:T(128)S(1)}, f32[128]{0:T(128)}, u32[]{:S(2)}) copy-start(f32[128]{0:T(128)} %param.28) | copy-start | bytes 1540
  190.8 103.6 %copy-start.5 = (bf16[512,256]{1,0:T(8,128)(2,1)S(1)}, bf16[512,256]{1,0:T(8,128)(2,1)}, u32[]{:S(2)}) copy-start(bf16[512,256]{1,0:T(8,128)(2,1)} %param.17) | copy-start | bytes 786436
Sparse Core Ops, SparseCore 0:
  9.4 93.8 all-gather.4
  114.5 71.6 all-gather.6
  246.3 48.1 all-gather.8
where the time goes:
time: 305 us; the launch traced here: 304 us
  waiting for transfers between devices  90.1 us (30%)
  blocking collectives  64.1 us (21%)
  matrix products  48.7 us (16%)
  starting transfers between devices  44.4 us (15%)
  local copies, waits for them, and re-layouts  22.5 us (7%)
  other arithmetic  19.2 us (6%)
  between operations  14.1 us (5%)
    all_gather x1, waiting for transfers between devices, local(): lax.all_gather(head_out, 'tp', axis=1, tiled=True)  48.3 us
    all_to_all x1, starting transfers between devices, sent_to_all(): lax.all_to_all(jnp.broadcast_to(value[None], (size, *value.shape)), axis,...  44.2 us
    all_gather x2, waiting for transfers between devices, in_one_piece(): lax.all_gather(both, axis, axis=dim, tiled=True)  41.6 us
    all_gather x1, blocking collectives, in_one_piece(): lax.all_gather(both, axis, axis=dim, tiled=True)  29.9 us
    dot_general x18, matrix products, absorb(): jnp.einsum('qhmk,khv->qhmv', exponent.astype(jnp.bfloat16), value_block,...  25.7 us
    all_gather x1, blocking collectives, local(): lax.all_gather(norm_gain, 'tp', axis=0, tiled=True)  18.9 us
    all_gather x1, blocking collectives, local(): lax.all_gather(modulation[:, :2], 'tp', axis=2, tiled=True)  15.3 us
    dynamic_slice x20, local copies, waits for them, and re-layouts, visit_block(): lax.dynamic_slice_in_dim(key_rows, first_row, block_rows, 0)  15 us
  transfers between devices with their start and end apart: 4, of which 3 were waited for; matrix products, arithmetic and copies ran while one was open for 5% of the time, Pallas kernels for 0%

commit v1 on v0

v1 whole, which is shorter than its diff:
```python
import functools

import jax
import jax.numpy as jnp
import numpy as np
from jax import lax
from jax.experimental import pallas as pl
from jax.experimental.pallas import tpu as pltpu
from jax.sharding import PartitionSpec as P

DK = 64
DV = 128
GRID_W = 64
EPS = 1e-06
LOG2E = 1.4426950408889634
MESH = pl.DeviceIdType.MESH
F32 = jnp.float32
BF16 = jnp.bfloat16


def angle_tables(grid_rows):
    half, quarter = DK // 2, DK // 4
    lane = np.arange(2 * DK) % DK
    inverse = (10000.0 ** (-2.0 * (lane % quarter) / half)).astype(np.float32)
    sign = np.where(lane % half < quarter, -1.0, 1.0).astype(np.float32)
    places = np.concatenate([np.arange(grid_rows), np.arange(GRID_W)]).astype(np.float32)
    angles = (places[:, None] * inverse[None, :]).astype(np.float32).astype(np.float64)
    return np.cos(angles).astype(np.float32), (np.sin(angles) * sign).astype(np.float32)


def kernel(
    nsp,
    ntp,
    latent,
    context,
    part,
    gain,
    w_query,
    w_key,
    w_value,
    query_gain,
    key_gain,
    lambdas,
    out_gain,
    w_out,
    cos_table,
    sin_table,
    out,
    feats,
    weights,
    w_mix,
    shares,
    pairs,
    squares,
    hid,
    proj,
    queries,
    kv,
    peak,
    total,
    blend,
    heads,
    mixed,
    load_sem,
    share_send,
    share_recv,
    pair_send,
    pair_recv,
    x_send,
    x_recv,
    d_send,
    d_recv,
    z_send,
    z_recv,
    o_send,
    o_recv,
    e_send,
    e_recv,
):
    me_sp, me_tp = lax.axis_index("sp"), lax.axis_index("tp")
    core, chip = lax.rem(me_tp, 2), lax.div(me_tp, 2)
    nchip = ntp // 2
    x_last, z_last = nchip // 2, nsp // 2
    partner = me_tp + 1 - 2 * core
    n_lat, cols = latent.shape
    n_ctx = context.shape[0]
    half = n_lat // 2
    offs, sizes = (0, half + n_ctx), (half + n_ctx, half)
    width = cols * ntp

    loads = [
        pltpu.make_async_copy(
            latent.at[pl.ds(0, half)], feats.at[me_tp, pl.ds(0, half)], load_sem.at[0]
        ),
        pltpu.make_async_copy(context, feats.at[me_tp, pl.ds(half, n_ctx)], load_sem.at[1]),
        pltpu.make_async_copy(
            latent.at[pl.ds(half, half)], feats.at[me_tp, pl.ds(offs[1], half)], load_sem.at[2]
        ),
        pltpu.make_async_copy(w_query, weights.at[:, :, pl.ds(0, 128)], load_sem.at[3]),
        pltpu.make_async_copy(w_key, weights.at[:, :, pl.ds(128, 128)], load_sem.at[4]),
        pltpu.make_async_copy(w_value, weights.at[:, :, pl.ds(256, 128)], load_sem.at[5]),
        pltpu.make_async_copy(w_out, w_mix, load_sem.at[6]),
    ]
    for load in loads:
        load.start()

    for at, (c, j) in enumerate(((0, 0), (0, 1), (1, 0), (1, 1), (0, 2))):
        shares[me_sp, :, at * cols : (at + 1) * cols] = part[c, j : j + 1, :]
    peak[...] = jnp.full(peak.shape, -1e30, F32)
    total[...] = jnp.zeros(total.shape, F32)
    blend[...] = jnp.zeros(blend.shape, F32)

    barrier = pltpu.get_barrier_semaphore()

    def greet_sp(k, carry):
        pl.semaphore_signal(
            barrier, 1, device_id={"sp": lax.rem(me_sp + k, nsp)}, device_id_type=MESH
        )
        return carry

    def greet_tp(k, carry):
        pl.semaphore_signal(
            barrier, 1, device_id={"tp": lax.rem(me_tp + k, ntp)}, device_id_type=MESH
        )
        return carry

    lax.fori_loop(1, nsp, greet_sp, 0)
    lax.fori_loop(1, ntp, greet_tp, 0)
    pl.semaphore_wait(barrier, nsp + ntp - 2)

    def share_copy(k, source):
        return pltpu.make_async_remote_copy(
            shares.at[source],
            shares.at[source],
            share_send.at[k],
            share_recv.at[k],
            device_id={"sp": lax.rem(me_sp + k, nsp)},
            device_id_type=MESH,
        )

    def pair_copy(k, source):
        return pltpu.make_async_remote_copy(
            pairs.at[source],
            pairs.at[source],
            pair_send.at[k],
            pair_recv.at[k],
            device_id={"tp": lax.rem(me_tp + k, ntp)},
            device_id_type=MESH,
        )

    def each(first, last, fn):
        def step(k, carry):
            fn(k)
            return carry

        lax.fori_loop(first, last, step, 0)

    each(1, nsp, lambda k: share_copy(k, me_sp).start())

    def place(h):
        return pl.ds(offs[h], sizes[h])

    def rows(h):
        return pl.ds(h * half, half)

    def tp_block(direction, step, which):
        there = chip - step if direction == 0 else chip + step
        return lax.rem(there + nchip, nchip) * 2 + which

    def ring_copy(buf, at, direction, step, h, send, recv):
        block = tp_block(direction, step - 1, core)
        target = me_tp + 2 if direction == 0 else me_tp + ntp - 2
        return pltpu.make_async_remote_copy(
            buf.at[block, at(h)],
            buf.at[block, at(h)],
            send.at[direction, step - 1, h],
            recv.at[direction, step - 1, h],
            device_id={"tp": lax.rem(target, ntp)},
            device_id_type=MESH,
        )

    def ring_arrival(buf, at, direction, step, h, send, recv):
        block = tp_block(direction, step, core)
        return pltpu.make_async_remote_copy(
            buf.at[block, at(h)],
            buf.at[block, at(h)],
            send.at[direction, step - 1, h],
            recv.at[direction, step - 1, h],
            device_id={"tp": partner},
            device_id_type=MESH,
        )

    def mate_copy(buf, at, direction, step, h, send, recv, which):
        block = tp_block(direction, step, which)
        slot = h if step == 0 else 2 + ((step - 1) * 2 + direction) * 2 + h
        return pltpu.make_async_remote_copy(
            buf.at[block, at(h)],
            buf.at[block, at(h)],
            send.at[slot],
            recv.at[slot],
            device_id={"tp": partner},
            device_id_type=MESH,
        )

    def has(direction, step, h, last):
        return step < last or (step == last and direction == h)

    def feature_step(step):
        for h in (0, 1):
            for d in (0, 1):
                if not has(d, step, h, x_last):
                    continue
                ring_arrival(feats, place, d, step, h, x_send, x_recv).wait_recv()
                if has(d, step + 1, h, x_last):
                    ring_copy(feats, place, d, step + 1, h, x_send, x_recv).start()
                mate_copy(feats, place, d, step, h, d_send, d_recv, core).start()

    for h in (0, 1):
        if h == 0:
            loads[0].wait()
            loads[1].wait()
        else:
            loads[2].wait()
        for d in (0, 1):
            ring_copy(feats, place, d, 1, h, x_send, x_recv).start()
        mate_copy(feats, place, 0, 0, h, d_send, d_recv, core).start()

    for step in range(1, x_last - 1):
        feature_step(step)

    each(1, nsp, lambda k: share_copy(k, lax.rem(me_sp + nsp - k, nsp)).wait_recv())
    modulation = jnp.sum(shares[...], axis=0)
    gate = modulation[:, 4 * cols : 5 * cols]
    gains = gain[...]
    pairs[me_tp, :, 0:cols] = modulation[:, 0:cols]
    pairs[me_tp, :, cols : 2 * cols] = gains * (1.0 + modulation[:, cols : 2 * cols])
    pairs[me_tp, :, 2 * cols : 3 * cols] = modulation[:, 2 * cols : 3 * cols]
    pairs[me_tp, :, 3 * cols : 4 * cols] = gains * (1.0 + modulation[:, 3 * cols : 4 * cols])
    each(1, ntp, lambda k: pair_copy(k, me_tp).start())

    for step in range(x_last - 1, x_last + 1):
        feature_step(step)

    for load in loads[3:6]:
        load.wait()
    each(1, ntp, lambda k: pair_copy(k, lax.rem(me_tp + ntp - k, ntp)).wait_recv())

    def z_block(direction, step):
        return lax.rem(me_sp + nsp + (2 * direction - 1) * step, nsp)

    def z_copy(direction, step, h):
        block = z_block(direction, step - 1)
        target = me_sp + 1 if direction == 0 else me_sp + nsp - 1
        return pltpu.make_async_remote_copy(
            kv.at[block, place(h)],
            kv.at[block, place(h)],
            z_send.at[direction, step - 1, h],
            z_recv.at[direction, step - 1, h],
            device_id={"sp": lax.rem(target, nsp)},
            device_id_type=MESH,
        )

    def z_arrival(direction, step, h):
        block = z_block(direction, step)
        target = me_sp + 1 if direction == 0 else me_sp + nsp - 1
        return pltpu.make_async_remote_copy(
            kv.at[block, place(h)],
            kv.at[block, place(h)],
            z_send.at[direction, step - 1, h],
            z_recv.at[direction, step - 1, h],
            device_id={"sp": lax.rem(target, nsp)},
            device_id_type=MESH,
        )

    lane = lax.broadcasted_iota(jnp.int32, (1, 2 * DK), 1)
    first_map = lane < DK
    by_row = lax.rem(lane, DK) < DK // 2
    lower = lax.rem(lane, DK // 2) < DK // 4
    grid_rows = half // GRID_W
    table_rows = nsp * 2 * grid_rows

    def head_norm(x, g):
        squared = x * x
        one = jnp.sum(jnp.where(first_map, squared, 0.0), axis=1, keepdims=True)
        two = jnp.sum(jnp.where(first_map, 0.0, squared), axis=1, keepdims=True)
        scale = jnp.where(
            first_map, lax.rsqrt(one * (1.0 / DK) + EPS), lax.rsqrt(two * (1.0 / DK) + EPS)
        )
        return x * scale * g

    def positions(table, h):
        mine = table[
            pl.ds(pl.multiple_of(me_sp * (2 * grid_rows), 2 * grid_rows), 2 * grid_rows), :
        ]
        columns = table[table_rows : table_rows + GRID_W, :]
        return jnp.concatenate(
            [
                jnp.where(by_row, mine[h * grid_rows + g : h * grid_rows + g + 1, :], columns)
                for g in range(grid_rows)
            ],
            axis=0,
        )

    def turn(x, cosine, sine):
        other = jnp.where(
            lower, pltpu.roll(x, 2 * DK - DK // 4, axis=1), pltpu.roll(x, DK // 4, axis=1)
        )
        return x * cosine + other * sine

    q_gain = jnp.concatenate([query_gain[...], query_gain[...]], axis=1) * (DK**-0.5 * LOG2E)
    k_gain = jnp.concatenate([key_gain[...], key_gain[...]], axis=1)

    def project(h):
        n = sizes[h]
        squares[...] = jnp.zeros(squares.shape, F32)

        def add_squares(b, carry):
            x = feats[b, offs[h] : offs[h] + n, :].astype(F32)
            y = x * x
            squares[0:n, :] += y[:, 0:128] + y[:, 128:256]
            return carry

        lax.fori_loop(0, ntp, add_squares, 0)
        factor = lax.rsqrt(
            jnp.sum(squares[0:n, :], axis=1, keepdims=True) * (1.0 / width) + EPS
        )
        squares[0:n, :] = jnp.broadcast_to(factor, (n, 128))
        proj[...] = jnp.zeros(proj.shape, F32)

        def add_block(b, carry):
            x = feats[b, offs[h] : offs[h] + half, :].astype(F32)
            f = jnp.concatenate([squares[0:half, :], squares[0:half, :]], axis=1)
            hid[0:half, :] = (
                x * f * pairs[b, :, cols : 2 * cols] + pairs[b, :, 0:cols]
            ).astype(BF16)
            if n > half:
                x = feats[b, offs[h] + half : offs[h] + n, :].astype(F32)
                f = jnp.concatenate([squares[half:n, :], squares[half:n, :]], axis=1)
                hid[half:n, :] = (
                    x * f * pairs[b, :, 3 * cols : 4 * cols] + pairs[b, :, 2 * cols : 3 * cols]
                ).astype(BF16)
            proj[0:n, :] += jnp.dot(hid[0:n, :], weights[b], preferred_element_type=F32)
            return carry

        lax.fori_loop(0, ntp, add_block, 0, unroll=2)
        cosine, sine = positions(cos_table, h), positions(sin_table, h)
        q = turn(head_norm(proj[0:half, 0:128], q_gain), cosine, sine)
        queries[h] = jnp.where(first_map, q, 0.0).astype(BF16)
        queries[2 + h] = jnp.where(first_map, 0.0, q).astype(BF16)
        k = turn(head_norm(proj[0:half, 128:256], k_gain), cosine, sine)
        kv[me_sp, offs[h] : offs[h] + half, 0:128] = k.astype(BF16)
        if n > half:
            kv[me_sp, offs[h] + half : offs[h] + n, 0:128] = head_norm(
                proj[half:n, 128:256], k_gain
            ).astype(BF16)
        kv[me_sp, offs[h] : offs[h] + n, 128:256] = proj[0:n, 256:384].astype(BF16)

    def mates(step_h, buf, at, send, recv):
        for step in range(0, x_last + 1):
            for d in (0, 1):
                if step == 0 and d == 1:
                    continue
                if step and not has(d, step, step_h, x_last):
                    continue
                mate_copy(buf, at, d, step, step_h, send, recv, 1 - core).wait_recv()

    for h in (0, 1):
        mates(h, feats, place, d_send, d_recv)
        project(h)
        for d in (0, 1):
            z_copy(d, 1, h).start()

    def absorb(block, h, chunks):
        n = sizes[h]
        keys = kv[block, offs[h] : offs[h] + n, 0:128]
        values = kv[block, offs[h] : offs[h] + n, 128:256]
        for c in chunks:
            scores = lax.dot_general(
                keys, queries[c], (((1,), (1,)), ((), ())), preferred_element_type=F32
            )
            old = peak[c]
            new = jnp.maximum(old, jnp.max(scores, axis=0, keepdims=True))
            expo = jnp.exp2(scores - new)
            rescale = jnp.exp2(old - new)
            total[c] = total[c] * rescale + jnp.sum(expo, axis=0, keepdims=True)
            blend[c] = blend[c] * rescale + lax.dot_general(
                values, expo.astype(BF16), (((0,), (0,)), ((), ())), preferred_element_type=F32
            )
            peak[c] = new

    for h in (0, 1):
        absorb(me_sp, h, range(4))

    def z_step(step, carry):
        for h in (0, 1):
            for d in (0, 1):
                z_arrival(d, step, h).wait_recv()
                if d == h:
                    z_copy(d, step + 1, h).start()
                else:

                    @pl.when(step < z_last - 1)
                    def _():
                        z_copy(d, step + 1, h).start()

            def both(d, inner):
                absorb(z_block(d, step), h, range(4))
                return inner

            lax.fori_loop(0, 2, both, 0)
        return carry

    lax.fori_loop(1, z_last, z_step, 0)
    for h in (0, 1):
        z_arrival(h, z_last, h).wait_recv()

    loads[6].wait()
    weight = lambdas[0]
    for h in (0, 1):
        for piece in (0, 1):
            absorb(z_block(piece, z_last), piece, (h, 2 + h))
        attended = blend[h] / total[h] - weight * (blend[2 + h] / total[2 + h])
        scale = lax.rsqrt(jnp.sum(attended * attended, axis=0, keepdims=True) * (1.0 / DV) + EPS)
        heads[me_tp, h * half : (h + 1) * half, :] = (
            jnp.transpose(attended * scale) * out_gain[...]
        ).astype(BF16)
        for d in (0, 1):
            ring_copy(heads, rows, d, 1, h, o_send, o_recv).start()
        mate_copy(heads, rows, 0, 0, h, e_send, e_recv, core).start()

    def mix(direction, step, h):
        mate_copy(heads, rows, direction, step, h, e_send, e_recv, 1 - core).wait_recv()
        first = tp_block(direction, step, 0)
        both = jnp.concatenate(
            [
                heads[first, h * half : (h + 1) * half, :],
                heads[first + 1, h * half : (h + 1) * half, :],
            ],
            axis=1,
        )
        piece = jnp.dot(both, w_mix[lax.div(first, 2)], preferred_element_type=F32)
        if step == 0:
            mixed[h * half : (h + 1) * half, :] = piece
        else:
            mixed[h * half : (h + 1) * half, :] += piece

    for h in (0, 1):
        mix(0, 0, h)
    for step in range(1, x_last + 1):
        for h in (0, 1):
            here = [d for d in (0, 1) if has(d, step, h, x_last)]
            for d in here:
                ring_arrival(heads, rows, d, step, h, o_send, o_recv).wait_recv()
                if has(d, step + 1, h, x_last):
                    ring_copy(heads, rows, d, step + 1, h, o_send, o_recv).start()
                mate_copy(heads, rows, d, step, h, e_send, e_recv, core).start()
            for d in here:
                mix(d, step, h)
            if step == x_last:
                mine = feats[me_tp, offs[h] : offs[h] + half, :].astype(F32)
                out[h * half : (h + 1) * half, :] = (
                    mine + gate * mixed[h * half : (h + 1) * half, :]
                ).astype(BF16)

    each(1, nsp, lambda k: share_copy(k, me_sp).wait_send())
    each(1, ntp, lambda k: pair_copy(k, me_tp).wait_send())
    for buf, at, send, recv, own_send, own_recv in (
        (feats, place, x_send, x_recv, d_send, d_recv),
        (heads, rows, o_send, o_recv, e_send, e_recv),
    ):
        for step in range(0, x_last + 1):
            for d in (0, 1):
                for h in (0, 1):
                    if step and has(d, step, h, x_last):
                        ring_copy(buf, at, d, step, h, send, recv).wait_send()
                    if (step and has(d, step, h, x_last)) or (step == 0 and d == 0):
                        mate_copy(buf, at, d, step, h, own_send, own_recv, core).wait_send()

    def z_sent(step, carry):
        for h in (0, 1):
            for d in (0, 1):
                z_copy(d, step, h).wait_send()
        return carry

    lax.fori_loop(1, z_last, z_sent, 0)
    for h in (0, 1):
        z_copy(h, z_last, h).wait_send()


def local(
    latent,
    context,
    conditions,
    mod_weight,
    norm_gain,
    w_query,
    w_key,
    w_value,
    query_gain,
    key_gain,
    lambdas,
    out_gain,
    w_out,
):
    nsp, ntp = lax.axis_size("sp"), lax.axis_size("tp")
    n_lat, cols = latent.shape
    n_ctx = context.shape[0]
    block = n_lat + n_ctx
    half = n_lat // 2
    nchip = ntp // 2
    activated = jax.nn.silu(conditions).astype(BF16)
    part = jnp.einsum("ci,ijn->cjn", activated, mod_weight, preferred_element_type=F32)
    cosine, sine = angle_tables(nsp * n_lat // GRID_W)
    vmem = pl.BlockSpec(memory_space=pltpu.VMEM)
    smem = pl.BlockSpec(memory_space=pltpu.SMEM)
    hbm = pl.BlockSpec(memory_space=pl.ANY)
    dma = pltpu.SemaphoreType.DMA
    return pl.pallas_call(
        functools.partial(kernel, nsp, ntp),
        out_shape=jax.ShapeDtypeStruct((n_lat, cols), BF16),
        in_specs=[hbm, hbm, vmem, vmem, hbm, hbm, hbm, vmem, vmem, smem, vmem, hbm, vmem, vmem],
        out_specs=vmem,
        scratch_shapes=[
            pltpu.VMEM((ntp, block, cols), BF16),
            pltpu.VMEM((ntp, cols, 3 * DV), BF16),
            pltpu.VMEM((nchip, 2 * DV, cols), BF16),
            pltpu.VMEM((nsp, 1, 5 * cols), F32),
            pltpu.VMEM((ntp, 1, 4 * cols), F32),
            pltpu.VMEM((half + n_ctx, 128), F32),
            pltpu.VMEM((half + n_ctx, cols), BF16),
            pltpu.VMEM((half + n_ctx, 3 * DV), F32),
            pltpu.VMEM((4, half, 2 * DK), BF16),
            pltpu.VMEM((nsp, block, 2 * DK + DV), BF16),
            pltpu.VMEM((4, 1, half), F32),
            pltpu.VMEM((4, 1, half), F32),
            pltpu.VMEM((4, DV, half), F32),
            pltpu.VMEM((ntp, n_lat, DV), BF16),
            pltpu.VMEM((n_lat, cols), F32),
            dma((7,)),
            dma((nsp,)),
            dma((nsp,)),
            dma((ntp,)),
            dma((ntp,)),
            dma((2, nchip // 2, 2)),
            dma((2, nchip // 2, 2)),
            dma((2 + 2 * nchip,)),
            dma((2 + 2 * nchip,)),
            dma((2, nsp // 2, 2)),
            dma((2, nsp // 2, 2)),
            dma((2, nchip // 2, 2)),
            dma((2, nchip // 2, 2)),
            dma((2 + 2 * nchip,)),
            dma((2 + 2 * nchip,)),
        ],
        compiler_params=pltpu.CompilerParams(collective_id=0, has_side_effects=True),
    )(
        latent,
        context,
        part,
        norm_gain[None],
        w_query.reshape(ntp, cols, DV),
        w_key.reshape(ntp, cols, DV),
        w_value.reshape(ntp, cols, DV),
        query_gain[None],
        key_gain[None],
        lambdas,
        out_gain[None],
        w_out.reshape(nchip, 2 * DV, cols),
        jnp.asarray(cosine),
        jnp.asarray(sine),
    )


def solution(mesh):
    in_specs = (
        P(("grp", "sp"), "tp"),
        P(("grp", "sp"), "tp"),
        P("grp", "sp"),
        P("sp", None, "tp"),
        P("tp"),
        P(None, "tp"),
        P(None, "tp"),
        P(None, "tp"),
        P(),
        P(),
        P("tp"),
        P(),
        P(None, "tp"),
    )
    out_specs = P(("grp", "sp"), "tp")
    return jax.shard_map(local, mesh=mesh, in_specs=in_specs, out_specs=out_specs, check_vma=False)
```

time: 305 us -> 157 us (0.51)
  Pallas kernels: 0 us -> 153 us
  waiting for transfers between devices: 90.1 us -> 0 us
  blocking collectives: 64.1 us -> 0 us
  matrix products: 48.7 us -> 0.17 us
  starting transfers between devices: 44.4 us -> 0 us
  local copies, waits for them, and re-layouts: 22.5 us -> 2.99 us
  other arithmetic: 19.2 us -> 0 us
  between operations: 14.1 us -> 0.72 us
    pallas_call x0 -> x1, Pallas kernels: none -> 153 us  [local(): pl.pallas_call(functools.partial(kernel, nsp, ntp), out_shape=jax.ShapeDt...]
    all_gather x3 -> x0, waiting for transfers between devices: 89.9 us -> none  [the longest x1 48.3 us: local(): lax.all_gather(head_out, 'tp', axis=1, tiled=True)]
    all_gather x3 -> x0, blocking collectives: 64.1 us -> none  [the longest x1 29.9 us: in_one_piece(): lax.all_gather(both, axis, axis=dim, tiled=True)]
    dot_general x43 -> x1, matrix products: 48.7 us -> 0.17 us  [local(): jnp.einsum('ci,ijn->cjn', activated, mod_weight, preferred_element_type=F32)]
    all_to_all x1 -> x0, starting transfers between devices: 44.2 us -> none  [sent_to_all(): lax.all_to_all(jnp.broadcast_to(value[None], (size, *value.shape)), axis,...]
    dynamic_slice x20 -> x0, local copies, waits for them, and re-layouts: 15 us -> none  [visit_block(): lax.dynamic_slice_in_dim(key_rows, first_row, block_rows, 0)]
    reduce_sum x25 -> x0, other arithmetic: 11.2 us -> none  [the longest x18 6.54 us: absorb(): totals = totals * rescale + jnp.sum(exponent, axis=-1)]
    slice x5 -> x0, local copies, waits for them, and re-layouts: 4.65 us -> none  [the longest x2 4.64 us: in_one_piece(): lax.slice_in_dim(whole, at, at + a.shape[along], axis=along)]
  transfers between devices with their start and end apart: 4 -> 0, of which waited for: 3 -> 0; matrix products, arithmetic and copies ran while one was open for 5% -> 0% of each run, Pallas kernels for 0% -> 0%
where the time goes in v1:
time: 157 us
  Pallas kernels  153 us (97%)
  local copies, waits for them, and re-layouts  2.99 us (2%)
    pallas_call x1, Pallas kernels, local(): pl.pallas_call(functools.partial(kernel, nsp, ntp), out_shape=jax.ShapeDt...  153 us

profile of v1, /device:TPU:65, one launch (start us, length us, event | category | flops | bytes accessed | tf_op | source)
XLA Modules:
  0.0 157.2 jit_solution(10272013125777762366)
XLA Ops:
  0.0 0.0 copy-start
  0.7 0.0 copy-start.1
  0.7 0.3 copy-done
  1.0 0.4 copy-done.1
  1.4 0.2 fusion.1
  1.6 0.6 copy.16.part
  2.2 153.3 %shard_map.145 = bf16[512,256]{1,0:T(8,128)(2,1)} custom-call(bf16[512,256]{1,0:T(8,128)(2,1)} %latent.1, bf16[64,256]{1,0:T(8,128)(2,1)} %context.1, f32[2,3,256]{2,1,0:T(4,128)} %copy.16.part, f32[1,256]{1,0:T(1,128)} %bitcast.16, bf16[16,256,128]{2,1,0:T(8,128)(2,1)} %bitcast.12, bf16[16,256,128]{2,1,0:T(8,128)(2,1)} %bitcast.13, ...), custom_call_target="tpu_custom_call" | custom-call | tf_op jit(solution)/shard_map/pallas_call | solution.py:518
  155.5 1.7 %copy.19 = bf16[512,256]{1,0:T(8,128)(2,1)} copy(bf16[512,256]{1,0:T(8,128)(2,1)} %shard_map.145) | data formatting | bytes 524288
Async XLA Ops:
  0.0 1.0 copy-start
  0.7 0.7 copy-start.1

commit v2 on v1

v2 whole, which is shorter than its diff:
```python
import functools

import jax
import jax.numpy as jnp
import numpy as np
from jax import lax
from jax.experimental import pallas as pl
from jax.experimental.pallas import tpu as pltpu
from jax.sharding import PartitionSpec as P

DK = 64
DV = 128
GRID_W = 64
EPS = 1e-06
LOG2E = 1.4426950408889634
MESH = pl.DeviceIdType.MESH
F32 = jnp.float32
BF16 = jnp.bfloat16


def angle_tables(grid_rows):
    half, quarter = DK // 2, DK // 4
    lane = np.arange(2 * DK) % DK
    inverse = (10000.0 ** (-2.0 * (lane % quarter) / half)).astype(np.float32)
    sign = np.where(lane % half < quarter, -1.0, 1.0).astype(np.float32)
    places = np.concatenate([np.arange(grid_rows), np.arange(GRID_W)]).astype(np.float32)
    angles = (places[:, None] * inverse[None, :]).astype(np.float32).astype(np.float64)
    return np.cos(angles).astype(np.float32), (np.sin(angles) * sign).astype(np.float32)


def kernel(
    nsp,
    ntp,
    latent,
    context,
    part,
    gain,
    w_query,
    w_key,
    w_value,
    query_gain,
    key_gain,
    lambdas,
    out_gain,
    w_out,
    cos_table,
    sin_table,
    out,
    feats,
    weights,
    w_mix,
    shares,
    pairs,
    factors,
    proj,
    queries,
    kv,
    peak,
    total,
    blend,
    heads,
    mixed,
    load_sem,
    share_send,
    share_recv,
    pair_send,
    pair_recv,
    x_send,
    x_recv,
    d_send,
    d_recv,
    z_send,
    z_recv,
    o_send,
    o_recv,
    e_send,
    e_recv,
):
    me_sp, me_tp = lax.axis_index("sp"), lax.axis_index("tp")
    core, chip = lax.rem(me_tp, 2), lax.div(me_tp, 2)
    nchip = ntp // 2
    x_last, z_last = nchip // 2, nsp // 2
    partner = me_tp + 1 - 2 * core
    n_lat, cols = latent.shape
    n_ctx = context.shape[0]
    half, quarter = n_lat // 2, n_lat // 4
    width = cols * ntp
    lead = GRID_W
    chunks = (
        (0, lead, n_ctx, 0),
        (lead + n_ctx, quarter, 0, lead),
        (lead + n_ctx + quarter, quarter, 0, lead + quarter),
        (lead + n_ctx + 2 * quarter, n_lat - lead - 2 * quarter, 0, lead + 2 * quarter),
    )
    pieces = range(4)

    loads = []

    def load(src, dst):
        loads.append(pltpu.make_async_copy(src, dst, load_sem.at[len(loads)]))
        loads[-1].start()

    load(latent.at[pl.ds(0, lead)], feats.at[me_tp, pl.ds(0, lead)])
    load(context, feats.at[me_tp, pl.ds(lead, n_ctx)])
    load(latent.at[pl.ds(lead, n_lat - lead)], feats.at[me_tp, pl.ds(lead + n_ctx, n_lat - lead)])
    load(w_query, weights.at[:, :, pl.ds(0, 128)])
    load(w_key, weights.at[:, :, pl.ds(128, 128)])
    load(w_value, weights.at[:, :, pl.ds(256, 128)])
    load(w_out, w_mix)

    for at, (c, j) in enumerate(((0, 0), (0, 1), (1, 0), (1, 1), (0, 2))):
        shares[me_sp, :, at * cols : (at + 1) * cols] = part[c, j : j + 1, :]

    barrier = pltpu.get_barrier_semaphore()

    def each(first, last, fn):
        def step(k, carry):
            fn(k)
            return carry

        lax.fori_loop(first, last, step, 0)

    def greet(axis, target):
        pl.semaphore_signal(barrier, 1, device_id={axis: target}, device_id_type=MESH)

    each(1, nsp, lambda k: greet("sp", lax.rem(me_sp + k, nsp)))
    each(1, ntp, lambda k: greet("tp", lax.rem(me_tp + k, ntp)))
    peak[...] = jnp.full(peak.shape, -1e30, F32)
    total[...] = jnp.zeros(total.shape, F32)
    blend[...] = jnp.zeros(blend.shape, F32)
    pl.semaphore_wait(barrier, nsp + ntp - 2)

    def share_copy(k, source):
        return pltpu.make_async_remote_copy(
            shares.at[source],
            shares.at[source],
            share_send.at[k],
            share_recv.at[k],
            device_id={"sp": lax.rem(me_sp + k, nsp)},
            device_id_type=MESH,
        )

    def pair_copy(k, source):
        return pltpu.make_async_remote_copy(
            pairs.at[source],
            pairs.at[source],
            pair_send.at[k],
            pair_recv.at[k],
            device_id={"tp": lax.rem(me_tp + k, ntp)},
            device_id_type=MESH,
        )

    each(1, nsp, lambda k: share_copy(k, me_sp).start())

    def place(c):
        return pl.ds(chunks[c][0], chunks[c][1] + chunks[c][2])

    def rows(c):
        return pl.ds(c * quarter, quarter)

    def tp_block(direction, step, which):
        return lax.rem(chip + nchip + (2 * direction - 1) * step, nchip) * 2 + which

    def z_block(direction, step):
        return lax.rem(me_sp + nsp + (2 * direction - 1) * step, nsp)

    class Ring:
        def __init__(self, buf, at, block, target, send, recv, last):
            self.buf, self.at, self.block, self.target = buf, at, block, target
            self.send, self.recv, self.last = send, recv, last

        def copy(self, direction, step, c, back=1):
            where = self.buf.at[self.block(direction, step - back), self.at(c)]
            return pltpu.make_async_remote_copy(
                where,
                where,
                self.send.at[direction, step - 1, c],
                self.recv.at[direction, step - 1, c],
                device_id=self.target(direction),
                device_id_type=MESH,
            )

        def begin(self, c):
            for d in (0, 1):
                self.copy(d, 1, c).start()

        def advance(self, step, c, after=None):
            for d in (0, 1):
                self.copy(d, step, c, back=0).wait_recv()
                if d == c % 2:
                    self.copy(d, step + 1, c).start()
                else:

                    @pl.when(step < self.last - 1)
                    def _():
                        self.copy(d, step + 1, c).start()

                if after is not None:
                    after(d, step, c)

        def finish(self, c, after=None):
            self.copy(c % 2, self.last, c, back=0).wait_recv()
            if after is not None:
                after(c % 2, self.last, c)

        def sent(self):
            def step_sent(step):
                for c in pieces:
                    for d in (0, 1):
                        self.copy(d, step, c).wait_send()

            each(1, self.last, step_sent)
            for c in pieces:
                self.copy(c % 2, self.last, c).wait_send()

    def tp_target(direction):
        return {"tp": lax.rem(me_tp + (2 if direction == 0 else ntp - 2), ntp)}

    def sp_target(direction):
        return {"sp": lax.rem(me_sp + (1 if direction == 0 else nsp - 1), nsp)}

    def own_block(direction, step):
        return tp_block(direction, step, core)

    x_ring = Ring(feats, place, own_block, tp_target, x_send, x_recv, x_last)
    z_ring = Ring(kv, place, z_block, sp_target, z_send, z_recv, z_last)
    o_ring = Ring(heads, rows, own_block, tp_target, o_send, o_recv, x_last)

    class Mate:
        def __init__(self, buf, at, send, recv):
            self.buf, self.at, self.send, self.recv = buf, at, send, recv

        def copy(self, direction, step, c, which):
            own = isinstance(step, int) and step == 0
            slot = c if own else 4 + ((step - 1) * 2 + direction) * 4 + c
            where = self.buf.at[tp_block(direction, step, which), self.at(c)]
            return pltpu.make_async_remote_copy(
                where,
                where,
                self.send.at[slot],
                self.recv.at[slot],
                device_id={"tp": partner},
                device_id_type=MESH,
            )

        def give(self, direction, step, c):
            self.copy(direction, step, c, core).start()

        def every(self, c, fn):
            fn(0, 0, c)

            def step_fn(step):
                for d in (0, 1):
                    fn(d, step, c)

            each(1, x_last, step_fn)
            fn(c % 2, x_last, c)

    x_mate = Mate(feats, place, d_send, d_recv)
    o_mate = Mate(heads, rows, e_send, e_recv)

    def begin_features(c):
        x_ring.begin(c)
        x_mate.give(0, 0, c)

    loads[0].wait()
    loads[1].wait()
    begin_features(0)
    loads[2].wait()
    begin_features(1)

    def first_features(step):
        x_ring.advance(step, 0, x_mate.give)
        x_ring.advance(step, 1, x_mate.give)

    def later_features(step):
        x_ring.advance(step, 2, x_mate.give)
        x_ring.advance(step, 3, x_mate.give)

    each(1, x_last, first_features)
    begin_features(2)
    begin_features(3)
    x_ring.finish(0, x_mate.give)
    x_ring.finish(1, x_mate.give)

    def measure(c):
        at, n = chunks[c][0], chunks[c][1] + chunks[c][2]
        x_mate.every(c, lambda d, step, c: x_mate.copy(d, step, c, 1 - core).wait_recv())

        def add_squares(b, carry):
            x = feats[b, at : at + n, :].astype(F32)
            y = x * x
            return carry + y[:, 0:128] + y[:, 128:256]

        squares = lax.fori_loop(0, ntp, add_squares, jnp.zeros((n, 128), F32))
        factor = lax.rsqrt(jnp.sum(squares, axis=1, keepdims=True) * (1.0 / width) + EPS)
        factors[at : at + n, :] = jnp.broadcast_to(factor, (n, 128))

    measure(0)
    measure(1)
    each(1, nsp, lambda k: share_copy(k, lax.rem(me_sp + nsp - k, nsp)).wait_recv())
    modulation = jnp.sum(shares[...], axis=0)
    gate = modulation[:, 4 * cols : 5 * cols]
    gains = gain[...]
    pairs[me_tp, :, 0:cols] = modulation[:, 0:cols]
    pairs[me_tp, :, cols : 2 * cols] = gains * (1.0 + modulation[:, cols : 2 * cols])
    pairs[me_tp, :, 2 * cols : 3 * cols] = modulation[:, 2 * cols : 3 * cols]
    pairs[me_tp, :, 3 * cols : 4 * cols] = gains * (1.0 + modulation[:, 3 * cols : 4 * cols])
    each(1, ntp, lambda k: pair_copy(k, me_tp).start())
    later_features(1)
    for one in loads[3:6]:
        one.wait()
    each(1, ntp, lambda k: pair_copy(k, lax.rem(me_tp + ntp - k, ntp)).wait_recv())

    lane = lax.broadcasted_iota(jnp.int32, (1, 2 * DK), 1)
    first_map = lane < DK
    by_row = lax.rem(lane, DK) < DK // 2
    lower = lax.rem(lane, DK // 2) < DK // 4
    grid_rows = n_lat // GRID_W
    table_rows = nsp * grid_rows

    def head_norm(x, g):
        squared = x * x
        one = jnp.sum(jnp.where(first_map, squared, 0.0), axis=1, keepdims=True)
        two = jnp.sum(jnp.where(first_map, 0.0, squared), axis=1, keepdims=True)
        scale = jnp.where(
            first_map, lax.rsqrt(one * (1.0 / DK) + EPS), lax.rsqrt(two * (1.0 / DK) + EPS)
        )
        return x * scale * g

    def positions(table, first, n):
        mine = table[pl.ds(pl.multiple_of(me_sp * grid_rows, grid_rows), grid_rows), :]
        columns = table[table_rows : table_rows + GRID_W, :]
        return jnp.concatenate(
            [
                jnp.where(by_row, mine[g : g + 1, :], columns)
                for g in range(first // GRID_W, (first + n) // GRID_W)
            ],
            axis=0,
        )

    def turn(x, cosine, sine):
        other = jnp.where(
            lower, pltpu.roll(x, 2 * DK - DK // 4, axis=1), pltpu.roll(x, DK // 4, axis=1)
        )
        return x * cosine + other * sine

    q_gain = jnp.concatenate([query_gain[...], query_gain[...]], axis=1) * (DK**-0.5 * LOG2E)
    k_gain = jnp.concatenate([key_gain[...], key_gain[...]], axis=1)

    def project(c):
        at, n_here, n_more, first = chunks[c]
        n = n_here + n_more
        proj[0:n, :] = jnp.zeros((n, 3 * DV), F32)

        def modulated(b, start, count, column):
            x = feats[b, at + start : at + start + count, :].astype(F32)
            f = factors[at + start : at + start + count, :]
            f = jnp.concatenate([f, f], axis=1)
            shift = pairs[b, :, column * cols : (column + 1) * cols]
            scale = pairs[b, :, (column + 1) * cols : (column + 2) * cols]
            return (x * f * scale + shift).astype(BF16)

        def add_block(b, carry):
            x = modulated(b, 0, n_here, 0)
            if n_more:
                x = jnp.concatenate([x, modulated(b, n_here, n_more, 2)], axis=0)
            proj[0:n, :] += jnp.dot(x, weights[b], preferred_element_type=F32)
            return carry

        lax.fori_loop(0, ntp, add_block, 0, unroll=4)
        cosine, sine = positions(cos_table, first, n_here), positions(sin_table, first, n_here)
        k = turn(head_norm(proj[0:n_here, 128:256], k_gain), cosine, sine)
        kv[me_sp, at : at + n_here, 0:128] = k.astype(BF16)
        if n_more:
            kv[me_sp, at + n_here : at + n, 0:128] = head_norm(
                proj[n_here:n, 128:256], k_gain
            ).astype(BF16)
        kv[me_sp, at : at + n, 128:256] = proj[0:n, 256:384].astype(BF16)
        q = turn(head_norm(proj[0:n_here, 0:128], q_gain), cosine, sine)
        queries[0, first : first + n_here, :] = jnp.where(first_map, q, 0.0).astype(BF16)
        queries[1, first : first + n_here, :] = jnp.where(first_map, 0.0, q).astype(BF16)
        z_ring.begin(c)

    def absorb(parts, h):
        for m in (0, 1):
            i = 2 * m + h
            q = queries[m, h * half : (h + 1) * half, :]
            scores = [
                lax.dot_general(
                    kv[block, chunks[c][0] : chunks[c][0] + chunks[c][1] + chunks[c][2], 0:128],
                    q,
                    (((1,), (1,)), ((), ())),
                    preferred_element_type=F32,
                )
                for block, c in parts
            ]
            old = peak[i]
            new = old
            for s in scores:
                new = jnp.maximum(new, jnp.max(s, axis=0, keepdims=True))
            rescale = jnp.exp2(old - new)
            summed, mixture = total[i] * rescale, blend[i] * rescale
            for (block, c), s in zip(parts, scores):
                expo = jnp.exp2(s - new)
                summed += jnp.sum(expo, axis=0, keepdims=True)
                mixture += lax.dot_general(
                    kv[block, chunks[c][0] : chunks[c][0] + chunks[c][1] + chunks[c][2], 128:256],
                    expo.astype(BF16),
                    (((0,), (0,)), ((), ())),
                    preferred_element_type=F32,
                )
            total[i], blend[i], peak[i] = summed, mixture, new

    def absorb_step(step, c):
        for h in (0, 1):
            absorb([(z_block(0, step), c), (z_block(1, step), c)], h)

    def z_step(step, c):
        z_ring.advance(step, c)
        absorb_step(step, c)

    project(0)
    project(1)
    later_features(2)
    later_features(3)
    z_ring.advance(1, 0)
    z_ring.advance(1, 1)
    x_ring.finish(2, x_mate.give)
    x_ring.finish(3, x_mate.give)
    measure(2)
    project(2)
    z_ring.advance(2, 0)
    z_ring.advance(2, 1)
    measure(3)
    project(3)
    z_ring.advance(3, 0)
    z_ring.advance(3, 1)
    for h in (0, 1):
        absorb([(me_sp, 0), (me_sp, 1)], h)
    for h in (0, 1):
        absorb([(me_sp, 2), (me_sp, 3)], h)

    def mingled(step):
        z_step(step, 2)
        z_step(step, 3)
        z_ring.advance(step + 3, 0)
        absorb_step(step, 0)
        z_ring.advance(step + 3, 1)
        absorb_step(step, 1)

    gap = 3
    each(1, z_last - gap, mingled)
    z_ring.finish(0)
    z_ring.finish(1)

    def trailing(step):
        z_step(step, 2)
        absorb_step(step, 0)
        z_step(step, 3)
        absorb_step(step, 1)

    each(z_last - gap, z_last, trailing)
    for h in (0, 1):
        absorb([(z_block(0, z_last), 0), (z_block(1, z_last), 1)], h)
    z_ring.finish(2)
    z_ring.finish(3)

    loads[6].wait()
    weight = lambdas[0]
    for h in (0, 1):
        absorb([(z_block(0, z_last), 2), (z_block(1, z_last), 3)], h)
        attended = blend[h] / total[h] - weight * (blend[2 + h] / total[2 + h])
        scale = lax.rsqrt(jnp.sum(attended * attended, axis=0, keepdims=True) * (1.0 / DV) + EPS)
        heads[me_tp, h * half : (h + 1) * half, :] = (
            jnp.transpose(attended * scale) * out_gain[...]
        ).astype(BF16)
        for c in (2 * h, 2 * h + 1):
            o_ring.begin(c)
            o_mate.give(0, 0, c)

    def mix(direction, step, c):
        o_mate.copy(direction, step, c, 1 - core).wait_recv()
        first = tp_block(direction, step, 0)
        at = c * quarter
        both = jnp.concatenate(
            [heads[first, at : at + quarter, :], heads[first + 1, at : at + quarter, :]], axis=1
        )
        piece = jnp.dot(both, w_mix[lax.div(first, 2)], preferred_element_type=F32)
        if isinstance(step, int) and step == 0:
            mixed[at : at + quarter, :] = piece
        else:
            mixed[at : at + quarter, :] += piece

    for c in pieces:
        mix(0, 0, c)

    def out_step(step):
        for c in pieces:
            o_ring.advance(step, c, o_mate.give)
        for c in pieces:
            for d in (0, 1):
                mix(d, step, c)

    each(1, x_last, out_step)
    for c in pieces:
        o_ring.finish(c, o_mate.give)
    for c in pieces:
        mix(c % 2, x_last, c)
        at = c * quarter
        for start, count in ((at, lead), (at + lead, quarter - lead)):
            shift = 0 if start < lead else n_ctx
            mine = feats[me_tp, start + shift : start + shift + count, :].astype(F32)
            out[start : start + count, :] = (
                mine + gate * mixed[start : start + count, :]
            ).astype(BF16)

    each(1, nsp, lambda k: share_copy(k, me_sp).wait_send())
    each(1, ntp, lambda k: pair_copy(k, me_tp).wait_send())
    for ring in (x_ring, z_ring, o_ring):
        ring.sent()
    for mate in (x_mate, o_mate):
        for c in pieces:
            mate.every(c, lambda d, step, c: mate.copy(d, step, c, core).wait_send())


def local(
    latent,
    context,
    conditions,
    mod_weight,
    norm_gain,
    w_query,
    w_key,
    w_value,
    query_gain,
    key_gain,
    lambdas,
    out_gain,
    w_out,
):
    nsp, ntp = lax.axis_size("sp"), lax.axis_size("tp")
    n_lat, cols = latent.shape
    n_ctx = context.shape[0]
    block = n_lat + n_ctx
    half = n_lat // 2
    nchip = ntp // 2
    activated = jax.nn.silu(conditions).astype(BF16)
    part = jnp.einsum("ci,ijn->cjn", activated, mod_weight, preferred_element_type=F32)
    cosine, sine = angle_tables(nsp * n_lat // GRID_W)
    vmem = pl.BlockSpec(memory_space=pltpu.VMEM)
    smem = pl.BlockSpec(memory_space=pltpu.SMEM)
    hbm = pl.BlockSpec(memory_space=pl.ANY)
    dma = pltpu.SemaphoreType.DMA
    return pl.pallas_call(
        functools.partial(kernel, nsp, ntp),
        out_shape=jax.ShapeDtypeStruct((n_lat, cols), BF16),
        in_specs=[hbm, hbm, vmem, vmem, hbm, hbm, hbm, vmem, vmem, smem, vmem, hbm, vmem, vmem],
        out_specs=vmem,
        scratch_shapes=[
            pltpu.VMEM((ntp, block, cols), BF16),
            pltpu.VMEM((ntp, cols, 3 * DV), BF16),
            pltpu.VMEM((nchip, 2 * DV, cols), BF16),
            pltpu.VMEM((nsp, 1, 5 * cols), F32),
            pltpu.VMEM((ntp, 1, 4 * cols), F32),
            pltpu.VMEM((block, 128), F32),
            pltpu.VMEM((block, 3 * DV), F32),
            pltpu.VMEM((2, n_lat, 2 * DK), BF16),
            pltpu.VMEM((nsp, block, 2 * DK + DV), BF16),
            pltpu.VMEM((4, 1, half), F32),
            pltpu.VMEM((4, 1, half), F32),
            pltpu.VMEM((4, DV, half), F32),
            pltpu.VMEM((ntp, n_lat, DV), BF16),
            pltpu.VMEM((n_lat, cols), F32),
            dma((7,)),
            dma((nsp,)),
            dma((nsp,)),
            dma((ntp,)),
            dma((ntp,)),
            dma((2, nchip // 2, 4)),
            dma((2, nchip // 2, 4)),
            dma((4 + 4 * nchip,)),
            dma((4 + 4 * nchip,)),
            dma((2, nsp // 2, 4)),
            dma((2, nsp // 2, 4)),
            dma((2, nchip // 2, 4)),
            dma((2, nchip // 2, 4)),
            dma((4 + 4 * nchip,)),
            dma((4 + 4 * nchip,)),
        ],
        compiler_params=pltpu.CompilerParams(collective_id=0, has_side_effects=True),
    )(
        latent,
        context,
        part,
        norm_gain[None],
        w_query.reshape(ntp, cols, DV),
        w_key.reshape(ntp, cols, DV),
        w_value.reshape(ntp, cols, DV),
        query_gain[None],
        key_gain[None],
        lambdas,
        out_gain[None],
        w_out.reshape(nchip, 2 * DV, cols),
        jnp.asarray(cosine),
        jnp.asarray(sine),
    )


def solution(mesh):
    in_specs = (
        P(("grp", "sp"), "tp"),
        P(("grp", "sp"), "tp"),
        P("grp", "sp"),
        P("sp", None, "tp"),
        P("tp"),
        P(None, "tp"),
        P(None, "tp"),
        P(None, "tp"),
        P(),
        P(),
        P("tp"),
        P(),
        P(None, "tp"),
    )
    out_specs = P(("grp", "sp"), "tp")
    return jax.shard_map(local, mesh=mesh, in_specs=in_specs, out_specs=out_specs, check_vma=False)
```

time: 157 us -> 162 us (1.032)
  Pallas kernels: 153 us -> 158 us
    pallas_call x1, Pallas kernels: 153 us -> 158 us  [local(): pl.pallas_call(functools.partial(kernel, nsp, ntp), out_shape=jax.ShapeDt...]
where the time goes in v2:
time: 162 us
  Pallas kernels  158 us (98%)
  local copies, waits for them, and re-layouts  2.99 us (2%)
    pallas_call x1, Pallas kernels, local(): pl.pallas_call(functools.partial(kernel, nsp, ntp), out_shape=jax.ShapeDt...  158 us

profile of v2, /device:TPU:65, one launch (start us, length us, event | category | flops | bytes accessed | tf_op | source)
XLA Modules:
  0.0 162.0 jit_solution(7490373603917327595)
XLA Ops:
  0.0 0.0 copy-start
  0.7 0.0 copy-start.1
  0.7 0.3 copy-done
  1.0 0.4 copy-done.1
  1.4 0.2 fusion.1
  1.6 0.6 copy.16.part
  2.2 158.2 %shard_map.145 = bf16[512,256]{1,0:T(8,128)(2,1)} custom-call(bf16[512,256]{1,0:T(8,128)(2,1)} %latent.1, bf16[64,256]{1,0:T(8,128)(2,1)} %context.1, f32[2,3,256]{2,1,0:T(4,128)} %copy.16.part, f32[1,256]{1,0:T(1,128)} %bitcast.16, bf16[16,256,128]{2,1,0:T(8,128)(2,1)} %bitcast.12, bf16[16,256,128]{2,1,0:T(8,128)(2,1)} %bitcast.13, ...), custom_call_target="tpu_custom_call" | custom-call | tf_op jit(solution)/shard_map/pallas_call | solution.py:555
  160.4 1.7 %copy.19 = bf16[512,256]{1,0:T(8,128)(2,1)} copy(bf16[512,256]{1,0:T(8,128)(2,1)} %shard_map.145) | data formatting | bytes 524288
Async XLA Ops:
  0.0 1.0 copy-start
  0.7 0.7 copy-start.1

commit v3 on v2

--- a/solution.py
+++ b/solution.py
@@ -33,7 +33,8 @@
     ntp,
     latent,
     context,
-    part,
+    conditions,
+    mod_weight,
     gain,
     w_query,
     w_key,
@@ -47,6 +48,7 @@
     sin_table,
     out,
     feats,
+    w_mod,
     weights,
     w_mix,
     shares,
@@ -94,6 +96,21 @@
     )
     pieces = range(4)
 
+    barrier = pltpu.get_barrier_semaphore()
+
+    def each(first, last, fn):
+        def step(k, carry):
+            fn(k)
+            return carry
+
+        lax.fori_loop(first, last, step, 0)
+
+    def greet(axis, target):
+        pl.semaphore_signal(barrier, 1, device_id={axis: target}, device_id_type=MESH)
+
+    each(1, ntp, lambda k: greet("tp", lax.rem(me_tp + k, ntp)))
+    each(1, nsp, lambda k: greet("sp", lax.rem(me_sp + k, nsp)))
+
     loads = []
 
     def load(src, dst):
@@ -103,28 +120,20 @@
     load(latent.at[pl.ds(0, lead)], feats.at[me_tp, pl.ds(0, lead)])
     load(context, feats.at[me_tp, pl.ds(lead, n_ctx)])
     load(latent.at[pl.ds(lead, n_lat - lead)], feats.at[me_tp, pl.ds(lead + n_ctx, n_lat - lead)])
+    load(mod_weight, w_mod)
     load(w_query, weights.at[:, :, pl.ds(0, 128)])
     load(w_key, weights.at[:, :, pl.ds(128, 128)])
     load(w_value, weights.at[:, :, pl.ds(256, 128)])
     load(w_out, w_mix)
 
-    for at, (c, j) in enumerate(((0, 0), (0, 1), (1, 0), (1, 1), (0, 2))):
-        shares[me_sp, :, at * cols : (at + 1) * cols] = part[c, j : j + 1, :]
-
-    barrier = pltpu.get_barrier_semaphore()
-
-    def each(first, last, fn):
-        def step(k, carry):
-            fn(k)
-            return carry
-
-        lax.fori_loop(first, last, step, 0)
-
-    def greet(axis, target):
-        pl.semaphore_signal(barrier, 1, device_id={axis: target}, device_id_type=MESH)
-
-    each(1, nsp, lambda k: greet("sp", lax.rem(me_sp + k, nsp)))
-    each(1, ntp, lambda k: greet("tp", lax.rem(me_tp + k, ntp)))
+    loads[3].wait()
+    given = conditions[...]
+    activated = (given / (1.0 + jnp.exp(-given))).astype(BF16)
+    for j in range(3):
+        share = jnp.dot(activated, w_mod[j], preferred_element_type=F32)
+        for c in (0, 1) if j < 2 else (0,):
+            at = 2 * c + j if j < 2 else 4
+            shares[me_sp, :, at * cols : (at + 1) * cols] = share[c : c + 1, :]
     peak[...] = jnp.full(peak.shape, -1e30, F32)
     total[...] = jnp.zeros(total.shape, F32)
     blend[...] = jnp.zeros(blend.shape, F32)
@@ -268,20 +277,10 @@
     begin_features(0)
     loads[2].wait()
     begin_features(1)
-
-    def first_features(step):
-        x_ring.advance(step, 0, x_mate.give)
-        x_ring.advance(step, 1, x_mate.give)
-
-    def later_features(step):
-        x_ring.advance(step, 2, x_mate.give)
-        x_ring.advance(step, 3, x_mate.give)
-
-    each(1, x_last, first_features)
     begin_features(2)
-    begin_features(3)
-    x_ring.finish(0, x_mate.give)
-    x_ring.finish(1, x_mate.give)
+
+    def features(step, c):
+        x_ring.advance(step, c, x_mate.give)
 
     def measure(c):
         at, n = chunks[c][0], chunks[c][1] + chunks[c][2]
@@ -296,8 +295,11 @@
         factor = lax.rsqrt(jnp.sum(squares, axis=1, keepdims=True) * (1.0 / width) + EPS)
         factors[at : at + n, :] = jnp.broadcast_to(factor, (n, 128))
 
-    measure(0)
-    measure(1)
+    for c in (0, 1, 2):
+        features(1, c)
+    for c in (0, 1, 2):
+        features(2, c)
+    features(3, 0)
     each(1, nsp, lambda k: share_copy(k, lax.rem(me_sp + nsp - k, nsp)).wait_recv())
     modulation = jnp.sum(shares[...], axis=0)
     gate = modulation[:, 4 * cols : 5 * cols]
@@ -307,10 +309,9 @@
     pairs[me_tp, :, 2 * cols : 3 * cols] = modulation[:, 2 * cols : 3 * cols]
     pairs[me_tp, :, 3 * cols : 4 * cols] = gains * (1.0 + modulation[:, 3 * cols : 4 * cols])
     each(1, ntp, lambda k: pair_copy(k, me_tp).start())
-    later_features(1)
-    for one in loads[3:6]:
-        one.wait()
-    each(1, ntp, lambda k: pair_copy(k, lax.rem(me_tp + ntp - k, ntp)).wait_recv())
+    features(3, 1)
+    features(3, 2)
+    begin_features(3)
 
     lane = lax.broadcasted_iota(jnp.int32, (1, 2 * DK), 1)
     first_map = lane < DK
@@ -382,13 +383,17 @@
         queries[1, first : first + n_here, :] = jnp.where(first_map, 0.0, q).astype(BF16)
         z_ring.begin(c)
 
-    def absorb(parts, h):
+    def piece(block, c, lanes):
+        at, n = chunks[c][0], chunks[c][1] + chunks[c][2]
+        return kv[block, at : at + n, lanes[0] : lanes[1]]
+
+    def absorb_half(parts, h):
         for m in (0, 1):
             i = 2 * m + h
             q = queries[m, h * half : (h + 1) * half, :]
             scores = [
                 lax.dot_general(
-                    kv[block, chunks[c][0] : chunks[c][0] + chunks[c][1] + chunks[c][2], 0:128],
+                    piece(block, c, (0, 2 * DK)),
                     q,
                     (((1,), (1,)), ((), ())),
                     preferred_element_type=F32,
@@ -405,72 +410,99 @@
                 expo = jnp.exp2(s - new)
                 summed += jnp.sum(expo, axis=0, keepdims=True)
                 mixture += lax.dot_general(
-                    kv[block, chunks[c][0] : chunks[c][0] + chunks[c][1] + chunks[c][2], 128:256],
+                    piece(block, c, (2 * DK, 2 * DK + DV)),
                     expo.astype(BF16),
                     (((0,), (0,)), ((), ())),
                     preferred_element_type=F32,
                 )
             total[i], blend[i], peak[i] = summed, mixture, new
 
-    def absorb_step(step, c):
+    def absorb(parts):
         for h in (0, 1):
-            absorb([(z_block(0, step), c), (z_block(1, step), c)], h)
-
-    def z_step(step, c):
-        z_ring.advance(step, c)
-        absorb_step(step, c)
-
+            absorb_half(parts, h)
+
+    def take(step, c):
+        absorb([(z_block(0, step), c), (z_block(1, step), c)])
+
+    move = z_ring.advance
+    x_ring.finish(0, x_mate.give)
+    x_ring.finish(1, x_mate.give)
+    measure(0)
+    for one in loads[4:7]:
+        one.wait()
+    each(1, ntp, lambda k: pair_copy(k, lax.rem(me_tp + ntp - k, ntp)).wait_recv())
     project(0)
+    x_ring.finish(2, x_mate.give)
+    measure(1)
+    features(1, 3)
     project(1)
-    later_features(2)
-    later_features(3)
-    z_ring.advance(1, 0)
-    z_ring.advance(1, 1)
-    x_ring.finish(2, x_mate.give)
-    x_ring.finish(3, x_mate.give)
     measure(2)
     project(2)
-    z_ring.advance(2, 0)
-    z_ring.advance(2, 1)
+    move(1, 0)
+    features(2, 3)
+    move(1, 1)
+    move(1, 2)
+    move(2, 0)
+    features(3, 3)
+    move(2, 1)
+    move(2, 2)
+    x_ring.finish(3, x_mate.give)
     measure(3)
     project(3)
-    z_ring.advance(3, 0)
-    z_ring.advance(3, 1)
-    for h in (0, 1):
-        absorb([(me_sp, 0), (me_sp, 1)], h)
-    for h in (0, 1):
-        absorb([(me_sp, 2), (me_sp, 3)], h)
-
-    def mingled(step):
-        z_step(step, 2)
-        z_step(step, 3)
-        z_ring.advance(step + 3, 0)
-        absorb_step(step, 0)
-        z_ring.advance(step + 3, 1)
-        absorb_step(step, 1)
-
-    gap = 3
-    each(1, z_last - gap, mingled)
-    z_ring.finish(0)
-    z_ring.finish(1)
-
-    def trailing(step):
-        z_step(step, 2)
-        absorb_step(step, 0)
-        z_step(step, 3)
-        absorb_step(step, 1)
-
-    each(z_last - gap, z_last, trailing)
-    for h in (0, 1):
-        absorb([(z_block(0, z_last), 0), (z_block(1, z_last), 1)], h)
-    z_ring.finish(2)
+    move(3, 0)
+    move(3, 1)
+    absorb([(me_sp, 0), (me_sp, 1)])
+    move(3, 2)
+    absorb([(me_sp, 2), (me_sp, 3)])
+    move(1, 3)
+    take(1, 0)
+    take(1, 1)
+    take(1, 2)
+
+    def mingled(j):
+        a, b = 4 + 2 * j, 2 + 3 * j
+        move(a, 0)
+        take(a - 2, 0)
+        move(a, 1)
+        take(a - 2, 1)
+        move(b, 3)
+        take(b - 1, 3)
+        move(a, 2)
+        take(a - 2, 2)
+        move(a + 1, 0)
+        take(a - 1, 0)
+        move(b + 1, 3)
+        take(b, 3)
+        move(a + 1, 1)
+        take(a - 1, 1)
+        move(a + 1, 2)
+        take(a - 1, 2)
+        move(b + 2, 3)
+        take(b + 1, 3)
+
+    rounds = z_last // 2 - 2
+    each(0, rounds, mingled)
+    early, late = 4 + 2 * rounds, 2 + 3 * rounds
+    for step in range(early, z_last):
+        for c in (0, 1, 2):
+            move(step, c)
+            take(step - 2, c)
+    for step in range(late, z_last):
+        move(step, 3)
+        take(step - 1, 3)
+    for c in (0, 1, 2):
+        take(z_last - 2, c)
+        z_ring.finish(c)
+        take(z_last - 1, c)
+    take(z_last - 1, 3)
+    absorb([(z_block(0, z_last), 0), (z_block(1, z_last), 1)])
     z_ring.finish(3)
 
-    loads[6].wait()
+    loads[7].wait()
     weight = lambdas[0]
     for h in (0, 1):
-        absorb([(z_block(0, z_last), 2), (z_block(1, z_last), 3)], h)
-        attended = blend[h] / total[h] - weight * (blend[2 + h] / total[2 + h])
+        absorb_half([(z_block(0, z_last), 2), (z_block(1, z_last), 3)], h)
+        attended = blend[h] * (1.0 / total[h]) - blend[2 + h] * (weight / total[2 + h])
         scale = lax.rsqrt(jnp.sum(attended * attended, axis=0, keepdims=True) * (1.0 / DV) + EPS)
         heads[me_tp, h * half : (h + 1) * half, :] = (
             jnp.transpose(attended * scale) * out_gain[...]
@@ -492,19 +524,24 @@
         else:
             mixed[at : at + quarter, :] += piece
 
-    for c in pieces:
-        mix(0, 0, c)
+    def mix_all(step):
+        for c in pieces:
+            for d in (0, 1):
+                mix(d, step, c)
 
     def out_step(step):
         for c in pieces:
             o_ring.advance(step, c, o_mate.give)
-        for c in pieces:
-            for d in (0, 1):
-                mix(d, step, c)
-
-    each(1, x_last, out_step)
+        mix_all(step - 1)
+
+    for c in pieces:
+        o_ring.advance(1, c, o_mate.give)
+    for c in pieces:
+        mix(0, 0, c)
+    each(2, x_last, out_step)
     for c in pieces:
         o_ring.finish(c, o_mate.give)
+    mix_all(x_last - 1)
     for c in pieces:
         mix(c % 2, x_last, c)
         at = c * quarter
@@ -545,8 +582,7 @@
     block = n_lat + n_ctx
     half = n_lat // 2
     nchip = ntp // 2
-    activated = jax.nn.silu(conditions).astype(BF16)
-    part = jnp.einsum("ci,ijn->cjn", activated, mod_weight, preferred_element_type=F32)
+    n_in = mod_weight.shape[0]
     cosine, sine = angle_tables(nsp * n_lat // GRID_W)
     vmem = pl.BlockSpec(memory_space=pltpu.VMEM)
     smem = pl.BlockSpec(memory_space=pltpu.SMEM)
@@ -555,10 +591,12 @@
     return pl.pallas_call(
         functools.partial(kernel, nsp, ntp),
         out_shape=jax.ShapeDtypeStruct((n_lat, cols), BF16),
-        in_specs=[hbm, hbm, vmem, vmem, hbm, hbm, hbm, vmem, vmem, smem, vmem, hbm, vmem, vmem],
+        in_specs=[hbm, hbm, vmem, hbm, vmem]
+        + [hbm, hbm, hbm, vmem, vmem, smem, vmem, hbm, vmem, vmem],
         out_specs=vmem,
         scratch_shapes=[
             pltpu.VMEM((ntp, block, cols), BF16),
+            pltpu.VMEM((3, n_in, cols), BF16),
             pltpu.VMEM((ntp, cols, 3 * DV), BF16),
             pltpu.VMEM((nchip, 2 * DV, cols), BF16),
             pltpu.VMEM((nsp, 1, 5 * cols), F32),
@@ -572,7 +610,7 @@
             pltpu.VMEM((4, DV, half), F32),
             pltpu.VMEM((ntp, n_lat, DV), BF16),
             pltpu.VMEM((n_lat, cols), F32),
-            dma((7,)),
+            dma((8,)),
             dma((nsp,)),
             dma((nsp,)),
             dma((ntp,)),
@@ -592,7 +630,8 @@
     )(
         latent,
         context,
-        part,
+        conditions,
+        jnp.transpose(mod_weight, (1, 0, 2)),
         norm_gain[None],
         w_query.reshape(ntp, cols, DV),
         w_key.reshape(ntp, cols, DV),

time: 162 us -> 154 us (0.951)
  Pallas kernels: 158 us -> 151 us
    pallas_call x1, Pallas kernels: 158 us -> 151 us  [local(): pl.pallas_call(functools.partial(kernel, nsp, ntp), out_shape=jax.ShapeDt...]
where the time goes in v3:
time: 154 us
  Pallas kernels  151 us (98%)
  local copies, waits for them, and re-layouts  1.67 us (1%)
    pallas_call x1, Pallas kernels, local(): pl.pallas_call(functools.partial(kernel, nsp, ntp), out_shape=jax.ShapeDt...  151 us

profile of v3, /device:TPU:65, one launch (start us, length us, event | category | flops | bytes accessed | tf_op | source)
XLA Modules:
  0.0 153.8 jit_solution(11666708566072711974)
XLA Ops:
  0.7 151.4 %shard_map.145 = bf16[512,256]{1,0:T(8,128)(2,1)} custom-call(bf16[512,256]{1,0:T(8,128)(2,1)} %latent.1, bf16[64,256]{1,0:T(8,128)(2,1)} %context.1, f32[2,256]{1,0:T(2,128)} %conditions.1, bf16[3,256,256]{2,1,0:T(8,128)(2,1)} %bitcast.13, f32[1,256]{1,0:T(1,128)} %bitcast.14, bf16[16,256,128]{2,1,0:T(8,128)(2,1)} %bitcast.9, ...), custom_call_target="tpu_custom_call" | custom-call | tf_op jit(solution)/shard_map/pallas_call | solution.py:591
  152.1 1.7 %copy.18 = bf16[512,256]{1,0:T(8,128)(2,1)} copy(bf16[512,256]{1,0:T(8,128)(2,1)} %shard_map.145) | data formatting | bytes 524288

commit v4 on v3

--- a/solution.py
+++ b/solution.py
@@ -92,7 +92,8 @@
         (0, lead, n_ctx, 0),
         (lead + n_ctx, quarter, 0, lead),
         (lead + n_ctx + quarter, quarter, 0, lead + quarter),
-        (lead + n_ctx + 2 * quarter, n_lat - lead - 2 * quarter, 0, lead + 2 * quarter),
+        (lead + n_ctx + 2 * quarter, quarter, 0, lead + 2 * quarter),
+        (lead + n_ctx + 3 * quarter, lead, 0, lead + 3 * quarter),
     )
     pieces = range(4)
 
@@ -174,9 +175,9 @@
         return lax.rem(me_sp + nsp + (2 * direction - 1) * step, nsp)
 
     class Ring:
-        def __init__(self, buf, at, block, target, send, recv, last):
+        def __init__(self, buf, at, block, target, send, recv, last, pieces):
             self.buf, self.at, self.block, self.target = buf, at, block, target
-            self.send, self.recv, self.last = send, recv, last
+            self.send, self.recv, self.last, self.pieces = send, recv, last, pieces
 
         def copy(self, direction, step, c, back=1):
             where = self.buf.at[self.block(direction, step - back), self.at(c)]
@@ -214,12 +215,12 @@
 
         def sent(self):
             def step_sent(step):
-                for c in pieces:
+                for c in self.pieces:
                     for d in (0, 1):
                         self.copy(d, step, c).wait_send()
 
             each(1, self.last, step_sent)
-            for c in pieces:
+            for c in self.pieces:
                 self.copy(c % 2, self.last, c).wait_send()
 
     def tp_target(direction):
@@ -231,17 +232,19 @@
     def own_block(direction, step):
         return tp_block(direction, step, core)
 
-    x_ring = Ring(feats, place, own_block, tp_target, x_send, x_recv, x_last)
-    z_ring = Ring(kv, place, z_block, sp_target, z_send, z_recv, z_last)
-    o_ring = Ring(heads, rows, own_block, tp_target, o_send, o_recv, x_last)
+    x_ring = Ring(feats, place, own_block, tp_target, x_send, x_recv, x_last, range(5))
+    z_ring = Ring(kv, place, z_block, sp_target, z_send, z_recv, z_last, range(5))
+    o_ring = Ring(heads, rows, own_block, tp_target, o_send, o_recv, x_last, pieces)
 
     class Mate:
-        def __init__(self, buf, at, send, recv):
+        def __init__(self, buf, at, send, recv, pieces):
             self.buf, self.at, self.send, self.recv = buf, at, send, recv
+            self.pieces = pieces
 
         def copy(self, direction, step, c, which):
             own = isinstance(step, int) and step == 0
-            slot = c if own else 4 + ((step - 1) * 2 + direction) * 4 + c
+            count = len(self.pieces)
+            slot = c if own else count + ((step - 1) * 2 + direction) * count + c
             where = self.buf.at[tp_block(direction, step, which), self.at(c)]
             return pltpu.make_async_remote_copy(
                 where,
@@ -265,8 +268,8 @@
             each(1, x_last, step_fn)
             fn(c % 2, x_last, c)
 
-    x_mate = Mate(feats, place, d_send, d_recv)
-    o_mate = Mate(heads, rows, e_send, e_recv)
+    x_mate = Mate(feats, place, d_send, d_recv, range(5))
+    o_mate = Mate(heads, rows, e_send, e_recv, pieces)
 
     def begin_features(c):
         x_ring.begin(c)
@@ -312,6 +315,7 @@
     features(3, 1)
     features(3, 2)
     begin_features(3)
+    begin_features(4)
 
     lane = lax.broadcasted_iota(jnp.int32, (1, 2 * DK), 1)
     first_map = lane < DK
@@ -362,14 +366,22 @@
             scale = pairs[b, :, (column + 1) * cols : (column + 2) * cols]
             return (x * f * scale + shift).astype(BF16)
 
-        def add_block(b, carry):
-            x = modulated(b, 0, n_here, 0)
-            if n_more:
-                x = jnp.concatenate([x, modulated(b, n_here, n_more, 2)], axis=0)
-            proj[0:n, :] += jnp.dot(x, weights[b], preferred_element_type=F32)
+        group = 4
+
+        def add_blocks(g, carry):
+            inputs = []
+            for b in range(group):
+                x = modulated(g * group + b, 0, n_here, 0)
+                if n_more:
+                    x = jnp.concatenate([x, modulated(g * group + b, n_here, n_more, 2)], axis=0)
+                inputs.append(x)
+            matrix = weights[pl.ds(g * group, group)].reshape(group * cols, 3 * DV)
+            proj[0:n, :] += jnp.dot(
+                jnp.concatenate(inputs, axis=1), matrix, preferred_element_type=F32
+            )
             return carry
 
-        lax.fori_loop(0, ntp, add_block, 0, unroll=4)
+        lax.fori_loop(0, ntp // group, add_blocks, 0)
         cosine, sine = positions(cos_table, first, n_here), positions(sin_table, first, n_here)
         k = turn(head_norm(proj[0:n_here, 128:256], k_gain), cosine, sine)
         kv[me_sp, at : at + n_here, 0:128] = k.astype(BF16)
@@ -435,73 +447,60 @@
     x_ring.finish(2, x_mate.give)
     measure(1)
     features(1, 3)
+    features(1, 4)
     project(1)
     measure(2)
     project(2)
     move(1, 0)
     features(2, 3)
+    features(2, 4)
     move(1, 1)
     move(1, 2)
+    features(3, 3)
     move(2, 0)
-    features(3, 3)
+    features(3, 4)
     move(2, 1)
+    x_ring.finish(3, x_mate.give)
     move(2, 2)
-    x_ring.finish(3, x_mate.give)
     measure(3)
     project(3)
+    x_ring.finish(4, x_mate.give)
     move(3, 0)
+    measure(4)
+    project(4)
     move(3, 1)
     absorb([(me_sp, 0), (me_sp, 1)])
     move(3, 2)
-    absorb([(me_sp, 2), (me_sp, 3)])
-    move(1, 3)
-    take(1, 0)
-    take(1, 1)
-    take(1, 2)
-
-    def mingled(j):
-        a, b = 4 + 2 * j, 2 + 3 * j
-        move(a, 0)
-        take(a - 2, 0)
-        move(a, 1)
-        take(a - 2, 1)
-        move(b, 3)
-        take(b - 1, 3)
-        move(a, 2)
-        take(a - 2, 2)
-        move(a + 1, 0)
-        take(a - 1, 0)
-        move(b + 1, 3)
-        take(b, 3)
-        move(a + 1, 1)
-        take(a - 1, 1)
-        move(a + 1, 2)
-        take(a - 1, 2)
-        move(b + 2, 3)
-        take(b + 1, 3)
-
-    rounds = z_last // 2 - 2
-    each(0, rounds, mingled)
-    early, late = 4 + 2 * rounds, 2 + 3 * rounds
-    for step in range(early, z_last):
-        for c in (0, 1, 2):
+    absorb([(me_sp, 2), (me_sp, 3), (me_sp, 4)])
+    others = [(step, c) for step in range(4, z_last + 1) for c in (0, 1, 2)]
+    lasts = [(step, c) for step in range(1, z_last) for c in (3, 4)]
+    order = []
+    while others or lasts:
+        order += others[:1] + lasts[:1]
+        others, lasts = others[1:], lasts[1:]
+    waiting = [(step, c) for step in (1, 2, 3) for c in (0, 1, 2)]
+
+    def take_some(count):
+        for _ in range(min(count, len(waiting))):
+            take(*waiting.pop(0))
+
+    take_some(3)
+    for step, c in order:
+        if step < z_last:
             move(step, c)
-            take(step - 2, c)
-    for step in range(late, z_last):
-        move(step, 3)
-        take(step - 1, 3)
-    for c in (0, 1, 2):
-        take(z_last - 2, c)
-        z_ring.finish(c)
-        take(z_last - 1, c)
-    take(z_last - 1, 3)
+            waiting.append((step, c))
+        else:
+            z_ring.finish(c)
+        take_some(2 if len(waiting) > 5 else 1)
+    take_some(len(waiting))
     absorb([(z_block(0, z_last), 0), (z_block(1, z_last), 1)])
     z_ring.finish(3)
+    z_ring.finish(4)
 
     loads[7].wait()
     weight = lambdas[0]
     for h in (0, 1):
-        absorb_half([(z_block(0, z_last), 2), (z_block(1, z_last), 3)], h)
+        absorb_half([(z_block(0, z_last), 2), (z_block(1, z_last), 3), (z_block(0, z_last), 4)], h)
         attended = blend[h] * (1.0 / total[h]) - blend[2 + h] * (weight / total[2 + h])
         scale = lax.rsqrt(jnp.sum(attended * attended, axis=0, keepdims=True) * (1.0 / DV) + EPS)
         heads[me_tp, h * half : (h + 1) * half, :] = (
@@ -524,24 +523,23 @@
         else:
             mixed[at : at + quarter, :] += piece
 
-    def mix_all(step):
-        for c in pieces:
-            for d in (0, 1):
-                mix(d, step, c)
+    def mix_both(step, c):
+        for d in (0, 1):
+            mix(d, step, c)
+
+    for c in pieces:
+        o_ring.advance(1, c, o_mate.give)
+        mix(0, 0, c)
 
     def out_step(step):
         for c in pieces:
             o_ring.advance(step, c, o_mate.give)
-        mix_all(step - 1)
-
-    for c in pieces:
-        o_ring.advance(1, c, o_mate.give)
-    for c in pieces:
-        mix(0, 0, c)
+            mix_both(step - 1, c)
+
     each(2, x_last, out_step)
     for c in pieces:
         o_ring.finish(c, o_mate.give)
-    mix_all(x_last - 1)
+        mix_both(x_last - 1, c)
     for c in pieces:
         mix(c % 2, x_last, c)
         at = c * quarter
@@ -557,7 +555,7 @@
     for ring in (x_ring, z_ring, o_ring):
         ring.sent()
     for mate in (x_mate, o_mate):
-        for c in pieces:
+        for c in mate.pieces:
             mate.every(c, lambda d, step, c: mate.copy(d, step, c, core).wait_send())
 
 
@@ -615,12 +613,12 @@
             dma((nsp,)),
             dma((ntp,)),
             dma((ntp,)),
-            dma((2, nchip // 2, 4)),
-            dma((2, nchip // 2, 4)),
-            dma((4 + 4 * nchip,)),
-            dma((4 + 4 * nchip,)),
-            dma((2, nsp // 2, 4)),
-            dma((2, nsp // 2, 4)),
+            dma((2, nchip // 2, 5)),
+            dma((2, nchip // 2, 5)),
+            dma((5 + 5 * nchip,)),
+            dma((5 + 5 * nchip,)),
+            dma((2, nsp // 2, 5)),
+            dma((2, nsp // 2, 5)),
             dma((2, nchip // 2, 4)),
             dma((2, nchip // 2, 4)),
             dma((4 + 4 * nchip,)),

time: 154 us -> 151 us (0.981)
  Pallas kernels: 151 us -> 149 us
    pallas_call x1, Pallas kernels: 151 us -> 149 us  [local(): pl.pallas_call(functools.partial(kernel, nsp, ntp), out_shape=jax.ShapeDt...]
where the time goes in v4:
time: 151 us
  Pallas kernels  149 us (99%)
  local copies, waits for them, and re-layouts  1.67 us (1%)
    pallas_call x1, Pallas kernels, local(): pl.pallas_call(functools.partial(kernel, nsp, ntp), out_shape=jax.ShapeDt...  149 us

profile of v4, /device:TPU:65, one launch (start us, length us, event | category | flops | bytes accessed | tf_op | source)
XLA Modules:
  0.0 150.9 jit_solution(11643492478723854818)
XLA Ops:
  0.7 148.6 %shard_map.145 = bf16[512,256]{1,0:T(8,128)(2,1)} custom-call(bf16[512,256]{1,0:T(8,128)(2,1)} %latent.1, bf16[64,256]{1,0:T(8,128)(2,1)} %context.1, f32[2,256]{1,0:T(2,128)} %conditions.1, bf16[3,256,256]{2,1,0:T(8,128)(2,1)} %bitcast.13, f32[1,256]{1,0:T(1,128)} %bitcast.14, bf16[16,256,128]{2,1,0:T(8,128)(2,1)} %bitcast.9, ...), custom_call_target="tpu_custom_call" | custom-call | tf_op jit(solution)/shard_map/pallas_call | solution.py:589
  149.3 1.7 %copy.18 = bf16[512,256]{1,0:T(8,128)(2,1)} copy(bf16[512,256]{1,0:T(8,128)(2,1)} %shard_map.145) | data formatting | bytes 524288
